TPU v7x, 256 devices: a whole 4x4x8 slice. The times are simulated.
256 devices in a mesh: sp: 64 (over z, y, core), tp: 4 (over x).
Axes of the slice: x: 4, y: 4, z: 8, core: 2. Of those that a mesh axis runs over, the one named last changes fastest.
Arguments:
- block_input: bfloat16 [65536, 2048], P('sp'), may hold values from -6 to 6
- out_grad: bfloat16 [65536, 2048], P('sp'), may hold values from -16 to 16
- w_value: bfloat16 [2048, 1024], P(None, 'tp'), may hold values from -0.125 to 0.125
- w_gate: bfloat16 [2048, 1024], P(None, 'tp'), may hold values from -0.125 to 0.125
- conv_taps: float32 [31, 1024], P(None, 'tp'), may hold values from -4 to 4
- norm_gain: float32 [1024], P('tp'), may hold values from 0.1 to 1.9
- norm_shift: float32 [1024], P('tp'), may hold values from -3 to 3
- w_proj: bfloat16 [1024, 2048], P('tp'), may hold values from -0.1875 to 0.1875
Outputs:
- input_grad: bfloat16 [65536, 2048], P('sp', 'tp')
- value_wgrad: float32 [2048, 1024], P('sp', 'tp')
- gate_wgrad: float32 [2048, 1024], P('sp', 'tp')
- proj_wgrad: float32 [1024, 2048], P('tp', 'sp')
- taps_grad: float32 [31, 1024], P(None, 'tp')
- gain_grad: float32 [1024], P('tp')
- shift_grad: float32 [1024], P('tp')
All inputs are finite; a program needn't handle non-finite values.
Results may differ from a plain program's by a relative error of at most 0.014.
Values may be sent and summed in bfloat16 or wider, within the bound.
A program may use at most 128 MiB of HBM per device.

v0:
```python
import math

import jax
import jax.numpy as jnp
from jax import lax
from jax.sharding import Mesh
from jax.sharding import PartitionSpec as P

CH = 1024
SP = ("sp_0", "sp_1", "sp_2")


EPS = 0.05


def from_behind(block, axis, distance):
    devices = range(lax.axis_size(axis))
    route = [(i - distance, i) for i in devices if i - distance in devices]
    return lax.ppermute(block, axis, route)


def sent_to_all(x, axis):
    length = lax.axis_size(axis)
    return lax.all_to_all(jnp.broadcast_to(x[None], (length, *x.shape)), axis, 0, 0, tiled=True)


def of_everyone(x, axis):
    return sent_to_all(x, axis).sum(axis=0)


def together(arrays, axis):
    ravelled, at, gathered = (jnp.concatenate([a.reshape(-1) for a in arrays]), 0, [])
    subtotal = of_everyone(ravelled, axis)
    for a in arrays:
        gathered.append(subtotal[at : at + a.size].reshape(a.shape))
        at += a.size
    return tuple(gathered)


def cut_along(x, dim, length):
    lengths = x.shape
    pieces = x.reshape(*lengths[:dim], length, lengths[dim] // length, *lengths[dim + 1 :])
    return jnp.moveaxis(pieces, dim, 0)


def sum_at_owner(x, axis, dim):
    pieces = cut_along(x, dim, lax.axis_size(axis))
    arrived = lax.all_to_all(pieces, axis, split_axis=0, concat_axis=0, tiled=True)
    return arrived.astype(jnp.float32).sum(axis=0)


def sum_by_axis(subtotal, axes):
    for axis in axes:
        subtotal = lax.psum_scatter(subtotal, axis, scatter_dimension=0, tiled=True)
    return subtotal


def right_product(left, right):
    return lax.dot_general(
        left, right, (((1,), (1,)), ((), ())), preferred_element_type=jnp.float32
    )


def column_product(left, right):
    return lax.dot_general(
        left, right, (((0,), (0,)), ((), ())), preferred_element_type=jnp.float32
    )


def shards(block_input, out_grad, w_value, w_gate, conv_taps, norm_gain, norm_shift, w_proj):
    tok_rows = block_input.shape[0]
    kernel_len = conv_taps.shape[0]
    reach_back = kernel_len - 1
    channels_dev = w_value.shape[1]
    loss_scale = 1.0 / math.sqrt(tok_rows * lax.axis_size(SP))
    value_proj = jnp.dot(block_input, w_value, preferred_element_type=jnp.float32).astype(
        jnp.bfloat16
    )
    gate_proj = jnp.dot(block_input, w_gate, preferred_element_type=jnp.float32).astype(
        jnp.bfloat16
    )
    gate_sigmoid = jax.nn.sigmoid(gate_proj.astype(jnp.float32))
    value_wide = value_proj.astype(jnp.float32)
    gated_input = (value_wide * gate_sigmoid).astype(jnp.bfloat16)
    earlier = from_behind(gated_input[tok_rows - reach_back :], SP, 1)
    extended = jnp.concatenate([earlier, gated_input], axis=0).astype(jnp.float32)
    filtered = jnp.zeros((tok_rows, channels_dev), jnp.float32)
    for tap_index in range(kernel_len):
        begin = reach_back - tap_index
        filtered = filtered + conv_taps[tap_index] * extended[begin : begin + tok_rows]
    row_sum, row_square = together(
        (jnp.sum(filtered, axis=1), jnp.sum(filtered * filtered, axis=1)), "tp"
    )
    row_mean = row_sum / CH
    row_var = row_square / CH - row_mean * row_mean
    row_scale = lax.rsqrt(row_var + EPS)
    normed = (filtered - row_mean[:, None]) * row_scale[:, None]
    activated = normed * norm_gain + norm_shift
    act_sigmoid = jax.nn.sigmoid(activated)
    mixer_out = (activated * act_sigmoid).astype(jnp.bfloat16)
    grad_mixed = right_product(out_grad, w_proj)
    grad_act = grad_mixed * act_sigmoid * (1.0 + activated * (1.0 - act_sigmoid))
    grad_normed = grad_act * norm_gain
    back_sum, back_cross = together(
        (jnp.sum(grad_normed, axis=1), jnp.sum(grad_normed * normed, axis=1)), "tp"
    )
    grad_filtered = row_scale[:, None] * (
        grad_normed - back_sum[:, None] / CH - normed * (back_cross[:, None] / CH)
    )
    gain_part = jnp.sum(grad_act * normed, axis=0)
    shift_part = jnp.sum(grad_act, axis=0)
    padded_grad = jnp.pad(grad_filtered, ((reach_back, reach_back), (0, 0)))
    grad_extended = jnp.zeros((tok_rows + reach_back, channels_dev), jnp.float32)
    taps_rows = []
    for tap_index in range(kernel_len):
        begin = reach_back - tap_index
        grad_extended = (
            grad_extended
            + conv_taps[tap_index] * padded_grad[tap_index : tap_index + tok_rows + reach_back]
        )
        taps_rows.append(jnp.sum(grad_filtered * extended[begin : begin + tok_rows], axis=0))
    taps_part = jnp.stack(taps_rows, axis=0)
    returned = from_behind(grad_extended[:reach_back], SP, -1)
    grad_glu = jnp.concatenate(
        [grad_extended[reach_back:tok_rows], grad_extended[tok_rows:] + returned], axis=0
    )
    grad_value = (grad_glu * gate_sigmoid).astype(jnp.bfloat16)
    grad_gate = (grad_glu * value_wide * gate_sigmoid * (1.0 - gate_sigmoid)).astype(jnp.bfloat16)
    grad_both = jnp.concatenate([grad_value, grad_gate], axis=1)
    small_taps, small_gain, small_shift = together((taps_part, gain_part, shift_part), SP)
    partial_input = right_product(grad_value, w_value) + right_product(grad_gate, w_gate)
    input_grad = sum_at_owner(partial_input.astype(jnp.bfloat16), "tp", 1).astype(jnp.bfloat16)
    summed = sum_by_axis(
        jnp.concatenate(
            [column_product(block_input, grad_both), column_product(out_grad, mixer_out)], axis=1
        ),
        SP,
    )
    weight_sum = summed[:, : 2 * channels_dev]
    proj_sum = summed[:, 2 * channels_dev :]
    value_wgrad = weight_sum[:, :channels_dev] * loss_scale
    gate_wgrad = weight_sum[:, channels_dev:] * loss_scale
    proj_wgrad = (proj_sum * loss_scale).T
    return (
        input_grad,
        value_wgrad,
        gate_wgrad,
        proj_wgrad,
        small_taps * loss_scale,
        small_gain * loss_scale,
        small_shift * loss_scale,
    )


def solution(mesh):
    finer = Mesh(mesh.devices.reshape(8, 4, 2, mesh.shape["tp"]), ("sp_0", "sp_1", "sp_2", "tp"))
    return jax.shard_map(
        shards,
        mesh=finer,
        in_specs=(
            P(SP, None),
            P(SP, None),
            P(None, "tp"),
            P(None, "tp"),
            P(None, "tp"),
            P("tp"),
            P("tp"),
            P("tp", None),
        ),
        out_specs=(
            P(SP, "tp"),
            P(SP, "tp"),
            P(SP, "tp"),
            P("tp", SP),
            P(None, "tp"),
            P("tp"),
            P("tp"),
        ),
        check_vma=False,
    )
```

profile of v0, /device:TPU:1, one launch (start us, length us, event | category | flops | bytes accessed | tf_op | source)
XLA Modules:
  0.0 216.7 jit_solution(6332317814926509826)
XLA Ops:
  7.2 3.9 %convolution_convert_fusion.1 = bf16[1024,256]{1,0:T(8,128)(2,1)S(1)} fusion(bf16[1024,2048]{1,0:T(8,128)(2,1)} %param.8, bf16[2048,256]{1,0:T(8,128)(2,1)} %param.10), kind=kOutput, calls=%fused_computation.15 | convolution fusion | flops 1074003968 | bytes 5767168 | tf_op jit(solution)/shard_map/dot_general | solution.py:76
  11.3 2.3 %fusion.6 = (bf16[1024,256]{1,0:T(8,128)(2,1)S(1)}, f32[1024,256]{1,0:T(8,128)}) fusion(bf16[1024,256]{1,0:T(8,128)(2,1)S(1)} %convolution_convert_fusion.1, bf16[1024,2048]{1,0:T(8,128)(2,1)S(1)} %copy-done.12, bf16[2048,256]{1,0:T(8,128)(2,1)S(1)} %copy-done), kind=kOutput, calls=%fused_computation.17 | convolution fusion | flops 1075838976 | bytes 7340032 | tf_op jit(solution)/shard_map/dot_general | solution.py:79
  13.6 4.6 %collective-permute-start = (bf16[30,256]{1,0:T(8,128)(2,1)S(1)}, bf16[30,256]{1,0:T(8,128)(2,1)S(1)}, u32[]{:S(2)}, u32[]{:S(2)}) collective-permute-start(bf16[30,256]{1,0:T(8,128)(2,1)S(1)} %slice.501), channel_id=1, source_target_pairs={{0,4},{4,8},{8,12},{12,16},{16,20},{20,24},{24,28},{28,32},{32,36}... | collective-permute-start | bytes 46088 | tf_op jit(solution)/shard_map/ppermute | solution.py:19
  19.1 4.5 %fusion.23 = (f32[1024]{0:T(1024)S(1)}, f32[1024]{0:T(1024)S(1)}, f32[1024,256]{1,0:T(8,128)S(1)}) fusion(f32[1054,256]{1,0:T(8,128)S(1)} %maximum_convert_fusion, f32[256]{0:T(256)S(1)} %bitcast.149, f32[256]{0:T(256)S(1)} %bitcast.151, f32[256]{0:T(256)S(1)} %bitcast.93, f32[256]{0:T(256)S(1)} %bitcast.95, f32[256]{0:T(256)S(1)} %bitcast.97, ...), kind=kLoop, calls=%fused_computation.92 | loop fusion | flops 16775168 | bytes 33594368 | tf_op jit(solution)/shard_map/reduce_sum | solution.py:92
  23.7 8.1 %all_to_all.23 = f32[4,1,2048]{2,1,0:T(1,128)S(1)} all-to-all(f32[4,1,2048]{2,1,0:T(1,128)S(1)} %broadcast_in_dim.6), channel_id=1, replica_groups=mesh['sp_0'=8,'sp_1'=4,'sp_2'=2,'tp'=4] {'tp'}, dimensions={0} | all-to-all | bytes 65536 | tf_op jit(solution)/shard_map/all_to_all | solution.py:24
  31.9 5.2 %multiply_reduce_fusion = (f32[256]{0:T(256)S(1)}, f32[1024]{0:T(1024)S(1)}, f32[1024]{0:T(1024)S(1)}, f32[256]{0:T(256)S(1)}, f32[1024,256]{1,0:T(8,128)}) fusion(f32[1024,256]{1,0:T(8,128)S(1)} %get-tuple-element.73, f32[1024]{0:T(1024)S(1)} %get-tuple-element.115, f32[1024]{0:T(1024)S(1)} %get-tuple-element.114, f32[256]{0:T(256)S(1)} %copy-done.10, ...), kind=kOutput, calls=%fused_computation.25 | convolution fusion | flops 1078720000 | bytes 7360512 | tf_op jit(solution)/shard_map/dot_general | solution.py:59
  37.1 6.7 %all_to_all.24 = f32[4,1,2048]{2,1,0:T(1,128)S(1)} all-to-all(f32[4,1,2048]{2,1,0:T(1,128)S(1)} %broadcast_in_dim.7), channel_id=1, replica_groups=mesh['sp_0'=8,'sp_1'=4,'sp_2'=2,'tp'=4] {'tp'}, dimensions={0} | all-to-all | bytes 65536 | tf_op jit(solution)/shard_map/all_to_all | solution.py:24
  43.9 4.4 %multiply_reduce_fusion.1 = (f32[256]{0:T(256)S(1)}, f32[256]{0:T(256)S(1)}, f32[256]{0:T(256)S(1)}, f32[256]{0:T(256)S(1)}, f32[256]{0:T(256)S(1)}, /*index=5*/...) fusion(f32[1054,256]{1,0:T(8,128)S(1)} %maximum_convert_fusion,, ...), kind=kLoop, calls=%fused_computation.26 | loop fusion | flops 11267584 | bytes 22055936 | tf_op jit(solution)/shard_map/reduce_sum | solution.py:121
  48.3 4.9 %multiply_add_fusion = f32[1054,256]{1,0:T(8,128)S(1)} fusion(f32[1024,256]{1,0:T(8,128)S(1)} %get-tuple-element.72, f32[256]{0:T(256)S(1)} %bitcast.150, f32[256]{0:T(256)S(1)} %bitcast.152, f32[256]{0:T(256)S(1)} %bitcast.94, f32[256]{0:T(256)S(1)} %bitcast.96, f32[256]{0:T(256)S(1)} %bitcast.98, f32[256]{0:T(256)S(1)} %bitcast.100, f32[256]{0:T(256)S(1)} %bitcast.102, ...), kind=kLoop, calls=%fused_computation.16 | loop fusion | flops 16459264 | bytes 2159616 | tf_op jit(solution)/shard_map/add | solution.py:118
  53.2 3.3 %collective-permute-start.1 = (f32[30,256]{1,0:T(8,128)S(1)}, f32[30,256]{1,0:T(8,128)S(1)}, u32[]{:S(2)}, u32[]{:S(2)}) collective-permute-start(f32[30,256]{1,0:T(8,128)S(1)} %slice.539), channel_id=1, source_target_pairs={{4,0},{8,4},{12,8},{16,12},{20,16},{24,20},{28,24},{32,28},{36,32}... | collective-permute-start | bytes 92168 | tf_op jit(solution)/shard_map/ppermute | solution.py:19
  58.1 3.4 %collective-permute-done.1 = f32[30,256]{1,0:T(8,128)S(1)} collective-permute-done((f32[30,256]{1,0:T(8,128)S(1)}, f32[30,256]{1,0:T(8,128)S(1)}, u32[]{:S(2)}, u32[]{:S(2)}) %collective-permute-start.1) | collective-permute-done | bytes 30752 | tf_op jit(solution)/shard_map/ppermute | solution.py:19
  62.0 2.4 %convolution_bitcast_fusion = f32[2048,512]{0,1:T(8,128)S(1)} fusion(bf16[1024,2048]{1,0:T(8,128)(2,1)S(1)} %copy-done.13, bf16[1024,256]{1,0:T(8,128)(2,1)S(1)} %get-tuple-element.74, bf16[1024,256]{1,0:T(8,128)(2,1)S(1)} %get-tuple-element.75), kind=kOutput, calls=%fused_computation.3 | convolution fusion | flops 2149580800 | bytes 9437184 | tf_op jit(solution)/shard_map/dot_general | solution.py:65
  64.4 3.1 %pad_maximum_fusion = f32[2048,768]{0,1:T(8,128)} fusion(f32[2048,256]{0,1:T(8,128)S(1)} %convolution_bitcast_fusion.1, f32[2048,512]{0,1:T(8,128)S(1)} %convolution_bitcast_fusion), kind=kLoop, calls=%fused_computation.1 | loop fusion | flops 1572864 | bytes 12582912 | tf_op jit(solution)/shard_map/concatenate | solution.py:134
  67.5 2.7 %fusion.27 = f32[1024,2048]{1,0:T(8,128)S(1)} fusion(bf16[1024,256]{1,0:T(8,128)(2,1)} %copy-done.3, bf16[2048,256]{1,0:T(8,128)(2,1)} %param.10), kind=kOutput, calls=%fused_computation.96 | convolution fusion | flops 1073741824 | bytes 9961472 | tf_op jit(solution)/shard_map/dot_general | solution.py:59
  71.6 2.5 %copy.52 = bf16[128,4,8,512]{3,2,0,1:T(8,128)(2,1)} copy(bf16[128,4,8,512]{3,2,1,0:T(8,128)(2,1)S(1)} %bitcast.89) | data formatting | bytes 8388608 | tf_op jit(solution)/shard_map/reshape | solution.py:42
  74.0 4.9 %all-to-all-start.2 = ((bf16[4,1024,512]{2,1,0:T(8,128)(2,1)}), bf16[4,1024,512]{2,1,0:T(8,128)(2,1)}, u32[]{:S(2)}, u32[]{:S(2)}) async-start(bf16[4,1024,512]{2,1,0:T(8,128)(2,1)} %bitcast.90), calls=%async_computation.2 | async-start | bytes 8388608 | tf_op jit(solution)/shard_map/all_to_all | solution.py:48
  78.9 1.8 multiply_reduce_fusion.19
  80.8 45.8 %all-to-all-done.2 = bf16[4,1024,512]{2,1,0:T(8,128)(2,1)} async-done(((bf16[4,1024,512]{2,1,0:T(8,128)(2,1)}), bf16[4,1024,512]{2,1,0:T(8,128)(2,1)}, u32[]{:S(2)}, u32[]{:S(2)}) %all-to-all-start.2) | async-done | bytes 4194336 | tf_op jit(solution)/shard_map/all_to_all | solution.py:48
  126.6 2.4 %broadcast_in_dim.8 = f32[64,1,8448]{2,1,0:T(1,128)} broadcast(f32[8448]{0:T(1024)S(1)} %pad_maximum_fusion.2), dimensions={2} | broadcast | bytes 2196480 | tf_op jit(solution)/shard_map/broadcast_in_dim | solution.py:24
  129.1 15.8 %all-to-all-start.3 = ((f32[64,1,8448]{2,1,0:T(1,128)}), f32[64,1,8448]{2,1,0:T(1,128)S(1)}, u32[]{:S(2)}, u32[]{:S(2)}) async-start(f32[64,1,8448]{2,1,0:T(1,128)} %broadcast_in_dim.8), calls=%async_computation.4 | async-start | bytes 4325376 | tf_op jit(solution)/shard_map/all_to_all | solution.py:24
  145.2 2.3 %copy.33 = f32[256,768]{1,0:T(8,128)} copy(f32[256,768]{0,1:T(8,128)} %reduce-scatter.8.cloned.1.call-done) | data formatting | bytes 1572864
  147.9 4.1 %reduce_sum.378 = bf16[1024,512]{1,0:T(8,128)(2,1)} reduce(bf16[4,1024,512]{2,1,0:T(8,128)(2,1)} %all-to-all-done.2, bf16[]{:T(256)} %constant.19.clone.1), dimensions={0}, to_apply=%region_6.0 | reduce | flops 1572864 | bytes 5242882 | tf_op jit(solution)/shard_map/reduce_sum | solution.py:49
  152.0 44.0 %all-to-all-done.3 = f32[64,1,8448]{2,1,0:T(1,128)S(1)} async-done(((f32[64,1,8448]{2,1,0:T(1,128)}), f32[64,1,8448]{2,1,0:T(1,128)S(1)}, u32[]{:S(2)}, u32[]{:S(2)}) %all-to-all-start.3) | async-done | bytes 2162720 | tf_op jit(solution)/shard_map/all_to_all | solution.py:24
  198.5 8.4 %reduce-scatter.12.cloned.1.call-done = f32[32,768]{1,0:T(8,128)} async-done(((f32[64,768]{1,0:T(8,128)}), f32[32,768]{1,0:T(8,128)}) %reduce-scatter.12.cloned.1.call-update) | async-done | bytes 98320
  (74 shorter events, 11.0 us)
Async XLA Ops:
  7.2 4.0 %copy-start = (bf16[2048,256]{1,0:T(8,128)(2,1)S(1)}, bf16[2048,256]{1,0:T(8,128)(2,1)}, u32[]{:S(2)}) copy-start(bf16[2048,256]{1,0:T(8,128)(2,1)} %param.11) | copy-start | bytes 3145732
  7.2 138.1 %reduce-scatter.8.cloned.1.call-start = ((), (), s32[]{:S(2)}) async-start(), calls=%async_computation.7 | async-start | bytes 7077888 | tf_op jit(solution)/shard_map/reduce_scatter | solution.py:54
  7.2 4.0 %copy-start.12 = (bf16[1024,2048]{1,0:T(8,128)(2,1)S(1)}, bf16[1024,2048]{1,0:T(8,128)(2,1)}, u32[]{:S(2)}) copy-start(bf16[1024,2048]{1,0:T(8,128)(2,1)} %param.8) | copy-start | bytes 12582916
  11.3 2.3 %copy-start.7 = (bf16[1024,256]{1,0:T(8,128)(2,1)}, bf16[1024,256]{1,0:T(8,128)(2,1)S(1)}, u32[]{:S(2)}) copy-start(bf16[1024,256]{1,0:T(8,128)(2,1)S(1)} %convolution_convert_fusion.1) | copy-start | bytes 1572868
  11.3 6.9 %copy-start.9 = (f32[31,256]{1,0:T(8,128)S(1)}, f32[31,256]{1,0:T(8,128)}, u32[]{:S(2)}) copy-start(f32[31,256]{1,0:T(8,128)} %param.12) | copy-start | bytes 95236
  13.6 5.4 %collective-permute-start = (bf16[30,256]{1,0:T(8,128)(2,1)S(1)}, bf16[30,256]{1,0:T(8,128)(2,1)S(1)}, u32[]{:S(2)}, u32[]{:S(2)}) collective-permute-start(bf16[30,256]{1,0:T(8,128)(2,1)S(1)} %slice.501), channel_id=1, source_target_pairs={{0,4},{4,8},{8,12},{12,16},{16,20},{20,24},{24,28},{28,32},{32,36}... | collective-permute-start | bytes 46088 | tf_op jit(solution)/shard_map/ppermute | solution.py:19
  19.1 12.8 %copy-start.10 = (f32[256]{0:T(256)S(1)}, f32[256]{0:T(256)}, u32[]{:S(2)}) copy-start(f32[256]{0:T(256)} %param.13) | copy-start | bytes 3076
  19.1 12.8 %copy-start.14 = (f32[256]{0:T(256)S(1)}, f32[256]{0:T(256)}, u32[]{:S(2)}) copy-start(f32[256]{0:T(256)} %param.14) | copy-start | bytes 3076
  23.7 13.5 %copy-start.1 = (f32[1024,256]{1,0:T(8,128)}, f32[1024,256]{1,0:T(8,128)S(1)}, u32[]{:S(2)}) copy-start(f32[1024,256]{1,0:T(8,128)S(1)} %get-tuple-element.73) | copy-start | bytes 3145732
  43.8 12.7 %copy-start.11 = (bf16[1024,2048]{1,0:T(8,128)(2,1)S(1)}, bf16[1024,2048]{1,0:T(8,128)(2,1)}, u32[]{:S(2)}) copy-start(bf16[1024,2048]{1,0:T(8,128)(2,1)} %param.9) | copy-start | bytes 12582916
  48.3 8.2 %copy-start.2 = (f32[1024,256]{1,0:T(8,128)S(1)}, f32[1024,256]{1,0:T(8,128)}, u32[]{:S(2)}) copy-start(f32[1024,256]{1,0:T(8,128)} %copy-done.1) | copy-start | bytes 3145732
  53.2 8.4 %collective-permute-start.1 = (f32[30,256]{1,0:T(8,128)S(1)}, f32[30,256]{1,0:T(8,128)S(1)}, u32[]{:S(2)}, u32[]{:S(2)}) collective-permute-start(f32[30,256]{1,0:T(8,128)S(1)} %slice.539), channel_id=1, source_target_pairs={{4,0},{8,4},{12,8},{16,12},{20,16},{24,20},{28,24},{32,28},{36,32}... | collective-permute-start | bytes 92168 | tf_op jit(solution)/shard_map/ppermute | solution.py:19
  58.0 3.6 %copy-start.6 = (f32[1024,256]{1,0:T(8,128)S(1)}, f32[1024,256]{1,0:T(8,128)}, u32[]{:S(2)}) copy-start(f32[1024,256]{1,0:T(8,128)} %get-tuple-element.117) | copy-start | bytes 3145732
  58.0 3.6 %copy-start.8 = (bf16[1024,256]{1,0:T(8,128)(2,1)S(1)}, bf16[1024,256]{1,0:T(8,128)(2,1)}, u32[]{:S(2)}) copy-start(bf16[1024,256]{1,0:T(8,128)(2,1)} %copy-done.7) | copy-start | bytes 1572868
  58.1 3.9 %copy-start.13 = (bf16[1024,2048]{1,0:T(8,128)(2,1)S(1)}, bf16[1024,2048]{1,0:T(8,128)(2,1)}, u32[]{:S(2)}) copy-start(bf16[1024,2048]{1,0:T(8,128)(2,1)} %param.8) | copy-start | bytes 12582916
  61.9 2.4 %copy-start.3 = (bf16[1024,256]{1,0:T(8,128)(2,1)}, bf16[1024,256]{1,0:T(8,128)(2,1)S(1)}, u32[]{:S(2)}) copy-start(bf16[1024,256]{1,0:T(8,128)(2,1)S(1)} %get-tuple-element.75) | copy-start | bytes 1572868
  62.0 2.4 %copy-start.4 = (bf16[1024,256]{1,0:T(8,128)(2,1)}, bf16[1024,256]{1,0:T(8,128)(2,1)S(1)}, u32[]{:S(2)}) copy-start(bf16[1024,256]{1,0:T(8,128)(2,1)S(1)} %get-tuple-element.74) | copy-start | bytes 1572868
  67.5 2.7 %copy-start.5 = (bf16[1024,256]{1,0:T(8,128)(2,1)S(1)}, bf16[1024,256]{1,0:T(8,128)(2,1)}, u32[]{:S(2)}) copy-start(bf16[1024,256]{1,0:T(8,128)(2,1)} %copy-done.4) | copy-start | bytes 1572868
  74.0 52.6 %all-to-all-start.2 = ((bf16[4,1024,512]{2,1,0:T(8,128)(2,1)}), bf16[4,1024,512]{2,1,0:T(8,128)(2,1)}, u32[]{:S(2)}, u32[]{:S(2)}) async-start(bf16[4,1024,512]{2,1,0:T(8,128)(2,1)} %bitcast.90), calls=%async_computation.2 | async-start | bytes 8388608 | tf_op jit(solution)/shard_map/all_to_all | solution.py:48
  129.1 66.9 %all-to-all-start.3 = ((f32[64,1,8448]{2,1,0:T(1,128)}), f32[64,1,8448]{2,1,0:T(1,128)S(1)}, u32[]{:S(2)}, u32[]{:S(2)}) async-start(f32[64,1,8448]{2,1,0:T(1,128)} %broadcast_in_dim.8), calls=%async_computation.4 | async-start | bytes 4325376 | tf_op jit(solution)/shard_map/all_to_all | solution.py:24
  144.9 52.4 %reduce-scatter.10.cloned.1.call-start = ((), (), s32[]{:S(2)}) async-start(), calls=%async_computation.8 | async-start | bytes 983040
  147.6 59.3 %reduce-scatter.12.cloned.1.call-start = ((), (), s32[]{:S(2)}) async-start(), calls=%async_computation.9 | async-start | bytes 294912
Sparse Core Ops, SparseCore 0:
  67.6 77.5 reduce-scatter.7
  148.2 25.8 reduce-scatter.9
  197.4 9.4 reduce-scatter.11
where the time goes:
time: 217 us
  waiting for transfers between devices  103 us (47%)
  starting transfers between devices  28.9 us (13%)
  other arithmetic  25.2 us (12%)
  matrix products  19.3 us (9%)
  blocking collectives  14.8 us (7%)
  between operations  14.2 us (7%)
  local copies, waits for them, and re-layouts  11.5 us (5%)
    all_to_all x1, waiting for transfers between devices, sum_at_owner(): lax.all_to_all(pieces, axis, split_axis=0, concat_axis=0, tiled=True)  45.8 us
    all_to_all x1, waiting for transfers between devices, sent_to_all(): lax.all_to_all(jnp.broadcast_to(x[None], (length, *x.shape)), axis, 0, 0,...  44 us
    all_to_all x1, starting transfers between devices, sent_to_all(): lax.all_to_all(jnp.broadcast_to(x[None], (length, *x.shape)), axis, 0, 0,...  15.8 us
    all_to_all x2, blocking collectives, sent_to_all(): lax.all_to_all(jnp.broadcast_to(x[None], (length, *x.shape)), axis, 0, 0,...  14.8 us
    dot_general x3, matrix products, right_product(): lax.dot_general(left, right, (((1,), (1,)), ((), ())), preferred_element_...  9.24 us
    unnamed x5, waiting for transfers between devices  8.47 us
    ppermute x2, starting transfers between devices, from_behind(): return lax.ppermute(block, axis, route)  7.87 us
    reduce_sum x2, other arithmetic, shards(): jnp.sum(grad_filtered * extended[begin:begin + tok_rows], axis=0)  6.2 us
  transfers between devices with their start and end apart: 7, of which 6 were waited for; matrix products, arithmetic and copies ran while one was open for 10% of the time, Pallas kernels for 0%

commit v1 on v0

--- a/solution.py
+++ b/solution.py
@@ -1,13 +1,18 @@
+import functools
 import math
 
 import jax
 import jax.numpy as jnp
 from jax import lax
-from jax.sharding import Mesh
+from jax.experimental import pallas as pl
+from jax.experimental.pallas import tpu as pltpu
 from jax.sharding import PartitionSpec as P
 
 CH = 1024
-SP = ("sp_0", "sp_1", "sp_2")
+SP = "sp"
+MESH = pl.DeviceIdType.MESH
+BF = jnp.bfloat16
+F32 = jnp.float32
 
 
 EPS = 0.05
@@ -37,24 +42,6 @@
     return tuple(gathered)
 
 
-def cut_along(x, dim, length):
-    lengths = x.shape
-    pieces = x.reshape(*lengths[:dim], length, lengths[dim] // length, *lengths[dim + 1 :])
-    return jnp.moveaxis(pieces, dim, 0)
-
-
-def sum_at_owner(x, axis, dim):
-    pieces = cut_along(x, dim, lax.axis_size(axis))
-    arrived = lax.all_to_all(pieces, axis, split_axis=0, concat_axis=0, tiled=True)
-    return arrived.astype(jnp.float32).sum(axis=0)
-
-
-def sum_by_axis(subtotal, axes):
-    for axis in axes:
-        subtotal = lax.psum_scatter(subtotal, axis, scatter_dimension=0, tiled=True)
-    return subtotal
-
-
 def right_product(left, right):
     return lax.dot_general(
         left, right, (((1,), (1,)), ((), ())), preferred_element_type=jnp.float32
@@ -65,6 +52,216 @@
     return lax.dot_general(
         left, right, (((0,), (0,)), ((), ())), preferred_element_type=jnp.float32
     )
+
+
+def rows_product(left, right):
+    return lax.dot_general(left, right, (((1,), (1,)), ((), ())), preferred_element_type=F32)
+
+
+def cols_product(left, right):
+    return lax.dot_general(left, right, (((0,), (0,)), ((), ())), preferred_element_type=F32)
+
+
+def back_kernel(
+    scale,
+    x, g, gb, mx, wv, wg, sm,
+    ig_out, v_out, g_out, p_out, sm_out,
+    part, own, got_a, got_b, got_c,
+    wbuf, got_w, s1, got_y, s2, got_z,
+    smb, sm_c, sm_y, sm_z,
+    xs, xr, cs, cr, ys, yr, zs, zr, ms, mr,
+):
+    s = lax.axis_index(SP)
+    t = lax.axis_index("tp")
+    c, y, z = s % 2, (s // 2) % 4, s // 8
+    right, left, far = (t + 1) % 4, (t + 3) % 4, (t + 2) % 4
+    half, cols = part.shape[2], part.shape[3]
+
+    def at_y(k):
+        return {SP: (z * 4 + (y + k) % 4) * 2 + c}
+
+    def at_z(k):
+        return {SP: (((z + k) % 8) * 4 + y) * 2 + c}
+
+    partner = {SP: s + 1 - 2 * c}
+    peers = [{"tp": (t + k) % 4} for k in (1, 2, 3)] + [partner]
+    peers += [at_y(k) for k in (1, 2, 3)] + [at_z(k) for k in range(1, 8)]
+    barrier = pltpu.get_barrier_semaphore()
+    for peer in peers:
+        pl.semaphore_signal(barrier, inc=1, device_id=peer, device_id_type=MESH)
+    pl.semaphore_wait(barrier, len(peers))
+
+    def send(src, dst, ssem, rsem, device):
+        copy = pltpu.make_async_remote_copy(
+            src_ref=src, dst_ref=dst, send_sem=ssem, recv_sem=rsem,
+            device_id=device, device_id_type=MESH,
+        )
+        copy.start()
+        return copy
+
+    sm_copy = send(sm, sm_c, ms.at[0], mr.at[0], partner)
+
+    def partial(block, h):
+        rows = pl.ds(h * half, half)
+        span = pl.ds(pl.multiple_of(block * cols, cols), cols)
+        return rows_product(gb[rows, 0:256], wv[span, :]) + rows_product(
+            gb[rows, 256:512], wg[span, :]
+        )
+
+    to_right, to_left = {"tp": right}, {"tp": left}
+    part[0, 0] = partial(far, 0).astype(BF)
+    a_r = send(part.at[0, 0], got_a.at[0], xs.at[0], xr.at[0], to_right)
+    part[0, 1] = partial(far, 1).astype(BF)
+    a_l = send(part.at[0, 1], got_a.at[1], xs.at[1], xr.at[1], to_left)
+    part[1, 1] = partial(right, 1).astype(BF)
+    b_r = send(part.at[1, 1], got_b.at[0], xs.at[2], xr.at[2], to_right)
+    part[2, 0] = partial(left, 0).astype(BF)
+    b_l = send(part.at[2, 0], got_b.at[1], xs.at[3], xr.at[3], to_left)
+
+    sm_copy.wait_recv()
+    smb[0] = sm[...] + sm_c[...]
+    sm_ys = [send(smb.at[0], sm_y.at[k - 1], ms.at[k], mr.at[k], at_y(k)) for k in (1, 2, 3)]
+
+    w_copies = []
+    for n in range(3):
+        source, right_side, off = (g, mx, 0) if n == 0 else (x, gb, (n - 1) * 256)
+
+        def weight_tile(zb, _, n=n, source=source, right_side=right_side, off=off):
+            span = pl.ds(pl.multiple_of(zb * 256, 256), 256)
+            tile = cols_product(source[:, span], right_side[:, off : off + 256])
+            wbuf[n, pl.ds(zb * 4, 4)] = tile.astype(BF).reshape(4, 2, 32, 256)
+            return 0
+
+        lax.fori_loop(0, 8, weight_tile, 0)
+        w_copies.append(
+            send(wbuf.at[n, :, 1 - c], got_w.at[n], cs.at[n], cr.at[n], partner)
+        )
+
+    y_copies = []
+    for n in range(3):
+        w_copies[n].wait_recv()
+
+        def pair_sum(zb, _, n=n):
+            rows = pl.ds(zb * 4, 4)
+            pair = wbuf[n, rows, c].astype(F32) + got_w[n, rows].astype(F32)
+            s1[n, zb] = pair.astype(BF)
+            return 0
+
+        lax.fori_loop(0, 8, pair_sum, 0)
+        y_copies.append(
+            [
+                send(s1.at[n, :, (y + k) % 4], got_y.at[n, k - 1], ys.at[n, k - 1],
+                     yr.at[n, k - 1], at_y(k))
+                for k in (1, 2, 3)
+            ]
+        )
+
+    part[1, 0] = partial(right, 0).astype(BF)
+    part[2, 1] = partial(left, 1).astype(BF)
+    own[0] = partial(t, 0)
+    own[1] = partial(t, 1)
+
+    for copy in sm_ys:
+        copy.wait_recv()
+    smb[1] = smb[0] + sm_y[0] + sm_y[1] + sm_y[2]
+    sm_zs = [
+        send(smb.at[1], sm_z.at[k - 1], ms.at[3 + k], mr.at[3 + k], at_z(k)) for k in range(1, 8)
+    ]
+
+    a_r.wait_recv()
+    part[1, 0] = (part[1, 0].astype(F32) + got_a[0].astype(F32)).astype(BF)
+    c_r = send(part.at[1, 0], got_c.at[0], xs.at[4], xr.at[4], to_right)
+    a_l.wait_recv()
+    part[2, 1] = (part[2, 1].astype(F32) + got_a[1].astype(F32)).astype(BF)
+    c_l = send(part.at[2, 1], got_c.at[1], xs.at[5], xr.at[5], to_left)
+
+    z_copies = []
+    for n in range(3):
+        for copy in y_copies[n]:
+            copy.wait_recv()
+        total = s1[n, :, y].astype(F32)
+        for k in range(3):
+            total = total + got_y[n, k].astype(F32)
+        s2[n] = total.astype(BF)
+        z_copies.append(
+            [
+                send(s2.at[n, (z + k) % 8], got_z.at[n, k - 1], zs.at[n, k - 1],
+                     zr.at[n, k - 1], at_z(k))
+                for k in range(1, 8)
+            ]
+        )
+
+    for copy in sm_zs:
+        copy.wait_recv()
+    total = smb[1]
+    for k in range(7):
+        total = total + sm_z[k]
+    sm_out[...] = total * scale
+
+    for n, out in enumerate((p_out, v_out, g_out)):
+        for copy in z_copies[n]:
+            copy.wait_recv()
+        total = s2[n, z].astype(F32)
+        for k in range(7):
+            total = total + got_z[n, k].astype(F32)
+        out[...] = total * scale
+
+    b_r.wait_recv()
+    own[1] = own[1] + got_b[0].astype(F32)
+    b_l.wait_recv()
+    own[0] = own[0] + got_b[1].astype(F32)
+    c_r.wait_recv()
+    ig_out[0:half] = (own[0] + got_c[0].astype(F32)).astype(BF)
+    c_l.wait_recv()
+    ig_out[half : 2 * half] = (own[1] + got_c[1].astype(F32)).astype(BF)
+
+    for copy in [a_r, a_l, b_r, b_l, c_r, c_l, sm_copy, *sm_ys, *sm_zs, *w_copies]:
+        copy.wait_send()
+    for copies in y_copies + z_copies:
+        for copy in copies:
+            copy.wait_send()
+
+
+def back(scale, x, g, gb, mx, wv, wg, sm):
+    dma = pltpu.SemaphoreType.DMA
+    vmem = pl.BlockSpec(memory_space=pltpu.VMEM)
+    return pl.pallas_call(
+        functools.partial(back_kernel, scale),
+        out_shape=(
+            jax.ShapeDtypeStruct((1024, 512), BF),
+            jax.ShapeDtypeStruct((32, 256), F32),
+            jax.ShapeDtypeStruct((32, 256), F32),
+            jax.ShapeDtypeStruct((32, 256), F32),
+            jax.ShapeDtypeStruct((40, 256), F32),
+        ),
+        in_specs=[vmem] * 7,
+        out_specs=(vmem,) * 5,
+        scratch_shapes=[
+            pltpu.VMEM((3, 2, 512, 512), BF),
+            pltpu.VMEM((2, 512, 512), F32),
+            pltpu.VMEM((2, 512, 512), BF),
+            pltpu.VMEM((2, 512, 512), BF),
+            pltpu.VMEM((2, 512, 512), BF),
+            pltpu.VMEM((3, 32, 2, 32, 256), BF),
+            pltpu.VMEM((3, 32, 32, 256), BF),
+            pltpu.VMEM((3, 8, 4, 32, 256), BF),
+            pltpu.VMEM((3, 3, 8, 32, 256), BF),
+            pltpu.VMEM((3, 8, 32, 256), BF),
+            pltpu.VMEM((3, 7, 32, 256), BF),
+            pltpu.VMEM((2, 40, 256), F32),
+            pltpu.VMEM((40, 256), F32),
+            pltpu.VMEM((3, 40, 256), F32),
+            pltpu.VMEM((7, 40, 256), F32),
+            dma((6,)), dma((6,)), dma((3,)), dma((3,)), dma((3, 3)), dma((3, 3)),
+            dma((3, 7)), dma((3, 7)), dma((11,)), dma((11,)),
+        ],
+        compiler_params=pltpu.CompilerParams(
+            collective_id=0, has_side_effects=True, vmem_limit_bytes=60 * 1024 * 1024
+        ),
+        cost_estimate=pl.CostEstimate(
+            flops=8_000_000_000, bytes_accessed=16_000_000, transcendentals=0
+        ),
+    )(x, g, gb, mx, wv, wg, sm)
 
 
 def shards(block_input, out_grad, w_value, w_gate, conv_taps, norm_gain, norm_shift, w_proj):
@@ -127,36 +324,27 @@
     grad_value = (grad_glu * gate_sigmoid).astype(jnp.bfloat16)
     grad_gate = (grad_glu * value_wide * gate_sigmoid * (1.0 - gate_sigmoid)).astype(jnp.bfloat16)
     grad_both = jnp.concatenate([grad_value, grad_gate], axis=1)
-    small_taps, small_gain, small_shift = together((taps_part, gain_part, shift_part), SP)
-    partial_input = right_product(grad_value, w_value) + right_product(grad_gate, w_gate)
-    input_grad = sum_at_owner(partial_input.astype(jnp.bfloat16), "tp", 1).astype(jnp.bfloat16)
-    summed = sum_by_axis(
-        jnp.concatenate(
-            [column_product(block_input, grad_both), column_product(out_grad, mixer_out)], axis=1
-        ),
-        SP,
-    )
-    weight_sum = summed[:, : 2 * channels_dev]
-    proj_sum = summed[:, 2 * channels_dev :]
-    value_wgrad = weight_sum[:, :channels_dev] * loss_scale
-    gate_wgrad = weight_sum[:, channels_dev:] * loss_scale
-    proj_wgrad = (proj_sum * loss_scale).T
+    small = jnp.concatenate(
+        [taps_part, gain_part[None], shift_part[None], jnp.zeros((7, channels_dev), F32)], axis=0
+    )
+    input_grad, value_wgrad, gate_wgrad, proj_rows, sums = back(
+        loss_scale, block_input, out_grad, grad_both, mixer_out, w_value, w_gate, small
+    )
     return (
         input_grad,
         value_wgrad,
         gate_wgrad,
-        proj_wgrad,
-        small_taps * loss_scale,
-        small_gain * loss_scale,
-        small_shift * loss_scale,
+        proj_rows.T,
+        sums[:kernel_len],
+        sums[kernel_len],
+        sums[kernel_len + 1],
     )
 
 
 def solution(mesh):
-    finer = Mesh(mesh.devices.reshape(8, 4, 2, mesh.shape["tp"]), ("sp_0", "sp_1", "sp_2", "tp"))
     return jax.shard_map(
         shards,
-        mesh=finer,
+        mesh=mesh,
         in_specs=(
             P(SP, None),
             P(SP, None),

time: 217 us -> 120 us (0.55)
  waiting for transfers between devices: 103 us -> 0.95 us
  Pallas kernels: 0 us -> 55.1 us
  starting transfers between devices: 28.9 us -> 7.87 us
  between operations: 14.2 us -> 0.88 us
  matrix products: 19.3 us -> 11 us
  other arithmetic: 25.2 us -> 18.3 us
    all_to_all x2 -> x0, waiting for transfers between devices: 89.8 us -> none  [the longest x1 45.8 us: sum_at_owner(): lax.all_to_all(pieces, axis, split_axis=0, concat_axis=0, tiled=True)]
    pallas_call x0 -> x1, Pallas kernels: none -> 55.1 us  [back(): pl.pallas_call(functools.partial(back_kernel, scale), out_shape=(jax.Shap...]
    all_to_all x2 -> x0, starting transfers between devices: 20.7 us -> none  [the longest x1 15.8 us: sent_to_all(): lax.all_to_all(jnp.broadcast_to(x[None], (length, *x.shape)), axis, 0, 0,...]
    unnamed x5 -> x0, waiting for transfers between devices: 8.47 us -> none
    dot_general x3 -> x1, matrix products: 9.24 us -> 4.87 us  [right_product(): lax.dot_general(left, right, (((1,), (1,)), ((), ())), preferred_element_...]
    reduce_sum x1 -> x0, other arithmetic: 4.11 us -> none  [sum_at_owner(): return arrived.astype(jnp.float32).sum(axis=0)]
    dot_general x2 -> x0, matrix products: 3.89 us -> none  [column_product(): lax.dot_general(left, right, (((0,), (0,)), ((), ())), preferred_element_...]
    ppermute x2, waiting for transfers between devices: 4.23 us -> 0.95 us  [from_behind(): return lax.ppermute(block, axis, route)]
  transfers between devices with their start and end apart: 7 -> 2, of which waited for: 6 -> 2; matrix products, arithmetic and copies ran while one was open for 10% -> 4% of each run, Pallas kernels for 0% -> 0%
where the time goes in v1:
time: 120 us; the launch traced here: 119 us
  Pallas kernels  55.1 us (46%)
  other arithmetic  18.3 us (15%)
  blocking collectives  14.8 us (12%)
  matrix products  11 us (9%)
  local copies, waits for them, and re-layouts  10.3 us (9%)
  starting transfers between devices  7.87 us (7%)
    pallas_call x1, Pallas kernels, back(): pl.pallas_call(functools.partial(back_kernel, scale), out_shape=(jax.Shap...  55.1 us
    all_to_all x2, blocking collectives, sent_to_all(): lax.all_to_all(jnp.broadcast_to(x[None], (length, *x.shape)), axis, 0, 0,...  14.8 us
    ppermute x2, starting transfers between devices, from_behind(): return lax.ppermute(block, axis, route)  7.87 us
    reduce_sum x2, other arithmetic, shards(): jnp.sum(grad_filtered * extended[begin:begin + tok_rows], axis=0)  6.08 us
    dot_general x1, matrix products, right_product(): lax.dot_general(left, right, (((1,), (1,)), ((), ())), preferred_element_...  4.87 us
    add x1, other arithmetic, shards(): grad_extended + conv_taps[tap_index] * padded_grad[tap_index:tap_index +...  4.86 us
    reduce_sum x1, other arithmetic, shards(): jnp.sum(filtered, axis=1)  4.51 us
    unnamed x24, local copies, waits for them, and re-layouts  4.39 us
  transfers between devices with their start and end apart: 2, of which 2 were waited for; matrix products, arithmetic and copies ran while one was open for 4% of the time, Pallas kernels for 0%

profile of v1, /device:TPU:1, one launch (start us, length us, event | category | flops | bytes accessed | tf_op | source)
XLA Modules:
  0.0 119.1 jit_solution(1154485221820056169)
XLA Ops:
  0.7 3.9 %convolution_convert_fusion.1 = bf16[1024,256]{1,0:T(8,128)(2,1)S(1)} fusion(bf16[1024,2048]{1,0:T(8,128)(2,1)} %x.3, bf16[2048,256]{1,0:T(8,128)(2,1)} %wv.1), kind=kOutput, calls=%fused_computation.10 | convolution fusion | flops 1074003968 | bytes 5767168 | tf_op jit(solution)/shard_map/dot_general | solution.py:273
  4.6 0.2 copy-done.8
  4.8 2.3 %fusion.6 = (bf16[1024,256]{1,0:T(8,128)(2,1)S(1)}, f32[1024,256]{1,0:T(8,128)}) fusion(bf16[1024,256]{1,0:T(8,128)(2,1)S(1)} %convolution_convert_fusion.1, bf16[1024,2048]{1,0:T(8,128)(2,1)S(1)} %copy-done.7, bf16[2048,256]{1,0:T(8,128)(2,1)S(1)} %copy-done.8), kind=kOutput, calls=%fused_computation.12 | convolution fusion | flops 1075838976 | bytes 7340032 | tf_op jit(solution)/shard_map/dot_general | solution.py:276
  7.1 4.6 %collective-permute-start = (bf16[30,256]{1,0:T(8,128)(2,1)S(1)}, bf16[30,256]{1,0:T(8,128)(2,1)S(1)}, u32[]{:S(2)}, u32[]{:S(2)}) collective-permute-start(bf16[30,256]{1,0:T(8,128)(2,1)S(1)} %slice.478), channel_id=1, source_target_pairs={{0,4},{4,8},{8,12},{12,16},{16,20},{20,24},{24,28},{28,32},{32,36}... | collective-permute-start | bytes 46088 | tf_op jit(solution)/shard_map/ppermute | solution.py:24
  11.7 0.8 collective-permute-done
  12.7 4.5 %fusion.13 = (f32[1024]{0:T(1024)S(1)}, f32[1024]{0:T(1024)S(1)}, f32[1024,256]{1,0:T(8,128)S(1)}) fusion(f32[1054,256]{1,0:T(8,128)S(1)} %maximum_convert_fusion, f32[256]{0:T(256)S(1)} %bitcast.132, f32[256]{0:T(256)S(1)} %bitcast.134, f32[256]{0:T(256)S(1)} %bitcast.76, f32[256]{0:T(256)S(1)} %bitcast.78, f32[256]{0:T(256)S(1)} %bitcast.80, ...), kind=kLoop, calls=%fused_computation.71 | loop fusion | flops 16775168 | bytes 33594368 | tf_op jit(solution)/shard_map/reduce_sum | solution.py:289
  17.2 8.1 %all_to_all.12 = f32[4,1,2048]{2,1,0:T(1,128)S(1)} all-to-all(f32[4,1,2048]{2,1,0:T(1,128)S(1)} %broadcast_in_dim.10), channel_id=1, replica_groups=mesh['sp'=64,'tp'=4] {'tp'}, dimensions={0} | all-to-all | bytes 65536 | tf_op jit(solution)/shard_map/all_to_all | solution.py:29
  25.4 4.9 %multiply_reduce_fusion = (f32[256]{0:T(256)S(1)}, f32[1024]{0:T(1024)S(1)}, f32[1024]{0:T(1024)S(1)}, f32[256]{0:T(256)S(1)}, bf16[1024,256]{1,0:T(8,128)(2,1)}, /*index=5*/f32[1024,256]{1,0:T(8,128)}) fusion(f32[1024,256]{1,0:T(8,128)S(1)} %get-tuple-element.55, f32[1024]{0:T(1024)S(1)} %get-tuple-element.95, f32[1024]{0:T(1024)S(1)} %get-tuple-element.94, ...), kind=kOutput, calls=%fused_computation.18 | convolution fusion | flops 1079244288 | bytes 7884800 | tf_op jit(solution)/shard_map/dot_general | solution.py:46
  30.3 6.7 %all_to_all.13 = f32[4,1,2048]{2,1,0:T(1,128)S(1)} all-to-all(f32[4,1,2048]{2,1,0:T(1,128)S(1)} %broadcast_in_dim.11), channel_id=1, replica_groups=mesh['sp'=64,'tp'=4] {'tp'}, dimensions={0} | all-to-all | bytes 65536 | tf_op jit(solution)/shard_map/all_to_all | solution.py:29
  37.0 4.3 %multiply_reduce_fusion.1 = (f32[256]{0:T(256)S(1)}, f32[256]{0:T(256)S(1)}, f32[256]{0:T(256)S(1)}, f32[256]{0:T(256)S(1)}, f32[256]{0:T(256)S(1)}, /*index=5*/...) fusion(f32[1054,256]{1,0:T(8,128)S(1)} %maximum_convert_fusion,, ...), kind=kLoop, calls=%fused_computation.19 | loop fusion | flops 11267584 | bytes 22055936 | tf_op jit(solution)/shard_map/reduce_sum | solution.py:318
  41.4 4.9 %multiply_add_fusion = f32[1054,256]{1,0:T(8,128)S(1)} fusion(f32[1024,256]{1,0:T(8,128)S(1)} %get-tuple-element.54, f32[256]{0:T(256)S(1)} %bitcast.133, f32[256]{0:T(256)S(1)} %bitcast.135, f32[256]{0:T(256)S(1)} %bitcast.77, f32[256]{0:T(256)S(1)} %bitcast.79, f32[256]{0:T(256)S(1)} %bitcast.81, f32[256]{0:T(256)S(1)} %bitcast.83, f32[256]{0:T(256)S(1)} %bitcast.85, ...), kind=kLoop, calls=%fused_computation.11 | loop fusion | flops 16459264 | bytes 2159616 | tf_op jit(solution)/shard_map/add | solution.py:315
  46.2 3.3 %collective-permute-start.1 = (f32[30,256]{1,0:T(8,128)S(1)}, f32[30,256]{1,0:T(8,128)S(1)}, u32[]{:S(2)}, u32[]{:S(2)}) collective-permute-start(f32[30,256]{1,0:T(8,128)S(1)} %slice.516), channel_id=1, source_target_pairs={{4,0},{8,4},{12,8},{16,12},{20,16},{24,20},{28,24},{32,28},{36,32}... | collective-permute-start | bytes 92168 | tf_op jit(solution)/shard_map/ppermute | solution.py:24
  49.5 1.8 %multiply_reduce_fusion.19 = (f32[256]{0:T(256)S(1)}, f32[256]{0:T(256)S(1)}, f32[256]{0:T(256)S(1)}, f32[256]{0:T(256)S(1)}, f32[256]{0:T(256)S(1)}, /*index=5*...) fusion(f32[1024,256]{1,0:T(8,128)S(1)} %get-tuple-element.54, ...), kind=kLoop, calls=%fused_computation.37 | loop fusion | flops 6812416 | bytes 14693376 | tf_op jit(solution)/shard_map/reduce_sum | solution.py:318
  51.4 3.0 %concatenate.23.sm = f32[40,256]{1,0:T(8,128)} concatenate(f32[1,256]{1,0:T(1,128)S(1)} %bitcast.166, f32[1,256]{1,0:T(1,128)S(1)} %bitcast.165, f32[1,256]{1,0:T(1,128)S(1)} %bitcast.164, f32[1,256]{1,0:T(1,128)S(1)} %bitcast.163, f32[1,256]{1,0:T(1,128)S(1)} %bitcast.162, f32[1,256]{1,0:T(1,128)S(1)} %bitcast.161, f32[1,256]{1,0:T(1,128)S(1)} %bitcast.160, ...), dimensions={0} | concatenate | bytes 81920 | tf_op jit(solution)/shard_map/concatenate | solution.py:327
  54.4 0.2 collective-permute-done.1
  54.6 1.6 %multiply_convert_fusion.1 = (bf16[1024,256]{1,0:T(8,128)(2,1)S(1)}, bf16[1024,256]{1,0:T(8,128)(2,1)S(1)}) fusion(f32[1024,256]{1,0:T(8,128)} %get-tuple-element.97, f32[30,256]{1,0:T(8,128)S(1)} %slice_add_fusion, f32[994,256]{1,0:T(8,128)S(1)} %slice.514, bf16[1024,256]{1,0:T(8,128)(2,1)} %copy-done.1), kind=kLoop, calls=%fused_computation.51 | loop fusion | flops 2359296 | bytes 3670016 | tf_op jit(solution)/shard_map/convert_element_type | solution.py:324
  56.2 1.1 pad_maximum_fusion.1.gb
  57.3 55.1 %shard_map.135 = (bf16[1024,512]{1,0:T(8,128)(2,1)}, f32[32,256]{1,0:T(8,128)}, f32[32,256]{1,0:T(8,128)}, f32[32,256]{1,0:T(8,128)}, f32[40,256]{1,0:T(8,128)}) custom-call(bf16[1024,2048]{1,0:T(8,128)(2,1)} %x.3, bf16[1024,2048]{1,0:T(8,128)(2,1)} %g.1, bf16[1024,512]{1,0:T(8,128)(2,1)} %pad_maximum_fusion.1.gb, bf16[1024,256]{1,0:T(8,128)(2,1)} %get-tuple-element.58.mx, ...), custom_call_target="tpu_custom_call" | custom-call | flops 8000000000 | bytes 16000000 | tf_op jit(solution)/shard_map/pallas_call | solution.py:228
  112.3 1.4 %slice.475 = f32[31,256]{1,0:T(8,128)} slice(f32[40,256]{1,0:T(8,128)} %get-tuple-element.16), slice={[0:31], [0:256]} | slice | bytes 63488 | tf_op jit(solution)/shard_map/slice | solution.py:338
  113.7 1.3 %fusion.14 = (f32[1,256]{1,0:T(1,128)}, f32[1,256]{1,0:T(1,128)}) fusion(f32[40,256]{1,0:T(8,128)} %get-tuple-element.16), kind=kLoop, calls=%fused_computation.72 | loop fusion | bytes 4096 | tf_op jit(solution)/shard_map/slice | solution.py:340
  115.0 2.3 %copy.27 = bf16[1024,512]{1,0:T(8,128)(2,1)} copy(bf16[1024,512]{1,0:T(8,128)(2,1)} %get-tuple-element.106) | data formatting | bytes 2097152
  117.3 0.6 copy.28
  117.9 0.6 copy.29
  118.5 0.6 copy.30
  (35 shorter events, 0.4 us)
Async XLA Ops:
  0.6 24.8 %copy-start = (bf16[256,2048]{1,0:T(8,128)(2,1)S(1)}, bf16[256,2048]{1,0:T(8,128)(2,1)}, u32[]{:S(2)}) copy-start(bf16[256,2048]{1,0:T(8,128)(2,1)} %param.15) | copy-start | bytes 3145732
  0.6 3.9 %copy-start.7 = (bf16[1024,2048]{1,0:T(8,128)(2,1)S(1)}, bf16[1024,2048]{1,0:T(8,128)(2,1)}, u32[]{:S(2)}) copy-start(bf16[1024,2048]{1,0:T(8,128)(2,1)} %x.3) | copy-start | bytes 12582916
  0.7 4.1 %copy-start.8 = (bf16[2048,256]{1,0:T(8,128)(2,1)S(1)}, bf16[2048,256]{1,0:T(8,128)(2,1)}, u32[]{:S(2)}) copy-start(bf16[2048,256]{1,0:T(8,128)(2,1)} %wg.1) | copy-start | bytes 3145732
  4.8 2.3 %copy-start.1 = (bf16[1024,256]{1,0:T(8,128)(2,1)}, bf16[1024,256]{1,0:T(8,128)(2,1)S(1)}, u32[]{:S(2)}) copy-start(bf16[1024,256]{1,0:T(8,128)(2,1)S(1)} %convolution_convert_fusion.1) | copy-start | bytes 1572868
  4.8 6.9 %copy-start.5 = (f32[31,256]{1,0:T(8,128)S(1)}, f32[31,256]{1,0:T(8,128)}, u32[]{:S(2)}) copy-start(f32[31,256]{1,0:T(8,128)} %param.12) | copy-start | bytes 95236
  7.1 5.4 %collective-permute-start = (bf16[30,256]{1,0:T(8,128)(2,1)S(1)}, bf16[30,256]{1,0:T(8,128)(2,1)S(1)}, u32[]{:S(2)}, u32[]{:S(2)}) collective-permute-start(bf16[30,256]{1,0:T(8,128)(2,1)S(1)} %slice.478), channel_id=1, source_target_pairs={{0,4},{4,8},{8,12},{12,16},{16,20},{20,24},{24,28},{28,32},{32,36}... | collective-permute-start | bytes 46088 | tf_op jit(solution)/shard_map/ppermute | solution.py:24
  12.6 12.8 %copy-start.6 = (f32[256]{0:T(256)S(1)}, f32[256]{0:T(256)}, u32[]{:S(2)}) copy-start(f32[256]{0:T(256)} %param.13) | copy-start | bytes 3076
  12.7 12.8 %copy-start.9 = (f32[256]{0:T(256)S(1)}, f32[256]{0:T(256)}, u32[]{:S(2)}) copy-start(f32[256]{0:T(256)} %param.14) | copy-start | bytes 3076
  46.2 8.4 %collective-permute-start.1 = (f32[30,256]{1,0:T(8,128)S(1)}, f32[30,256]{1,0:T(8,128)S(1)}, u32[]{:S(2)}, u32[]{:S(2)}) collective-permute-start(f32[30,256]{1,0:T(8,128)S(1)} %slice.516), channel_id=1, source_target_pairs={{4,0},{8,4},{12,8},{16,12},{20,16},{24,20},{28,24},{32,28},{36,32}... | collective-permute-start | bytes 92168 | tf_op jit(solution)/shard_map/ppermute | solution.py:24
  112.3 4.9 %copy-start.4 = (f32[32,256]{1,0:T(8,128)S(1)}, f32[32,256]{1,0:T(8,128)}, u32[]{:S(2)}) copy-start(f32[32,256]{1,0:T(8,128)} %get-tuple-element.107) | copy-start | bytes 98308
  115.0 2.9 %copy-start.3 = (f32[32,256]{1,0:T(8,128)S(1)}, f32[32,256]{1,0:T(8,128)}, u32[]{:S(2)}) copy-start(f32[32,256]{1,0:T(8,128)} %get-tuple-element.108) | copy-start | bytes 98308
  115.0 3.5 %copy-start.2 = (f32[32,256]{1,0:T(8,128)S(1)}, f32[32,256]{1,0:T(8,128)}, u32[]{:S(2)}) copy-start(f32[32,256]{1,0:T(8,128)} %get-tuple-element.15) | copy-start | bytes 98308

commit v2 on v0

v2 whole, which is shorter than its diff:
```python
import functools
import math

import jax
import jax.numpy as jnp
from jax import lax
from jax.experimental import pallas as pl
from jax.experimental.pallas import tpu as pltpu
from jax.sharding import PartitionSpec as P

CH = 1024
SP = "sp"
MESH = pl.DeviceIdType.MESH
BF = jnp.bfloat16
F32 = jnp.float32
EPS = 0.05
TAPS = 31
T = 256
TILES = 4
R = 64


def plain(left, right):
    return jnp.dot(left, right, preferred_element_type=F32)


def rows_product(left, right):
    return lax.dot_general(left, right, (((1,), (1,)), ((), ())), preferred_element_type=F32)


def cols_product(left, right):
    return lax.dot_general(left, right, (((0,), (0,)), ((), ())), preferred_element_type=F32)


def loop(count, body):
    def step(i, carry):
        body(i)
        return carry

    lax.fori_loop(0, count, step, 0)


def whole(
    scale,
    x_h, g_h, wv_h, wg_h, taps, gain, shift, wp_h,
    ig_out, w_out, sm_out,
    x, g, wv, wg, wp, load,
    gi, gi_halo, vf, sg, filt, gm, gf, gf_halo, gb, mx, tg, gs,
    stc, wide, col_a, col_b, st1, got1, st2, got2,
    part, own, got_a, got_b, got_c,
    wbuf, got_w, s1, got_y, s2, got_z,
    smb, sm_c, sm_y, sm_z,
    hs, hr, t1s, t1r, t2s, t2r, as_, ar, bs, br, cs, cr,
    ws, wr, ys, yr, zs, zr, ms, mr,
):
    s = lax.axis_index(SP)
    t = lax.axis_index("tp")
    c, y, z = s % 2, (s // 2) % 4, s // 8
    right, left, far = (t + 1) % 4, (t + 3) % 4, (t + 2) % 4
    last_sp = 63

    def local(src, dst, k):
        return pltpu.make_async_copy(src, dst, load.at[k])

    def x_rows(i):
        rows = pl.ds(i * T, T)
        return local(x_h.at[rows], x.at[rows], i)

    loads = [local(wv_h, wv, 4), local(wg_h, wg, 5)]
    loads[0].start()
    x_rows(3).start()
    loads[1].start()
    for i in range(3):
        x_rows(i).start()
    late = [local(wp_h, wp, 6), local(g_h, g, 7)]
    for copy in late:
        copy.start()

    def at_y(k):
        return {SP: (z * 4 + (y + k) % 4) * 2 + c}

    def at_z(k):
        return {SP: (((z + k) % 8) * 4 + y) * 2 + c}

    def at_t(k):
        return {"tp": (t + k) % 4}

    partner = {SP: s + 1 - 2 * c}
    after = {SP: (s + 1) % 64}
    before = {SP: (s + 63) % 64}
    peers = [at_t(k) for k in (1, 2, 3)] + [partner, after, before]
    peers += [at_y(k) for k in (1, 2, 3)] + [at_z(k) for k in range(1, 8)]
    barrier = pltpu.get_barrier_semaphore()
    for peer in peers:
        pl.semaphore_signal(barrier, inc=1, device_id=peer, device_id_type=MESH)

    def remote(src, dst, ssem, rsem, device):
        return pltpu.make_async_remote_copy(
            src_ref=src, dst_ref=dst, send_sem=ssem, recv_sem=rsem,
            device_id=device, device_id_type=MESH,
        )

    lane = lax.broadcasted_iota(jnp.int32, (R, 128), 1)
    tg[...] = jnp.zeros_like(tg)
    gs[...] = jnp.zeros_like(gs)
    wide[...] = jnp.zeros_like(wide)

    halo_send = remote(gi.at[:, pl.ds(1024, 32)], gi_halo, hs.at[0], hr.at[0], after)
    grad_send = remote(gf.at[:, pl.ds(0, 32)], gf_halo, hs.at[1], hr.at[1], before)

    def st1_send(i, k):
        return remote(st1.at[i], got1.at[i, k - 1], t1s.at[i, k - 1], t1r.at[i, k - 1], at_t(k))

    def st2_send(i, k):
        return remote(st2.at[i], got2.at[i, k - 1], t2s.at[i, k - 1], t2r.at[i, k - 1], at_t(k))

    def project(i):
        rows = pl.ds(pl.multiple_of(i * T, T), T)
        x_rows(i).wait()
        value = plain(x[rows, :], wv[...]).astype(BF).astype(F32)
        gate = plain(x[rows, :], wg[...]).astype(BF).astype(F32)
        sig = jax.nn.sigmoid(gate)
        gated = (value * sig).astype(BF).astype(F32)
        at = pl.ds(pl.multiple_of(i * T + 32, 32), T)
        for h in range(2):
            lanes = slice(h * 128, h * 128 + 128)
            vf[h, rows, :] = value[:, lanes]
            sg[h, rows, :] = sig[:, lanes]
            gi[h, at, :] = gated[:, lanes]

    for copy in loads:
        copy.wait()
    project(3)
    pl.semaphore_wait(barrier, len(peers))
    halo_send.start()
    loop(3, project)
    halo_send.wait_recv()
    gi[:, 0:32, :] = jnp.where(s == 0, 0.0, gi_halo[...])

    def filter_tile(i):
        def block(b):
            base = pl.multiple_of(i * T + b * R, R)
            out = []
            for h in range(2):
                acc = jnp.zeros((R, 128), F32)
                for k in range(TAPS):
                    tap = taps[k : k + 1, h * 128 : h * 128 + 128]
                    acc = acc + tap * gi[h, pl.ds(base + 32 - k, R), :]
                filt[h, pl.ds(base, R), :] = acc
                out.append(acc)
            total = jnp.sum(out[0] + out[1], axis=1, keepdims=True)
            square = jnp.sum(out[0] * out[0] + out[1] * out[1], axis=1, keepdims=True)
            stc[pl.ds(pl.multiple_of(b * R, R), R), :] = jnp.where(
                lane == 0, total, jnp.where(lane == 1, square, 0.0)
            )

        loop(T // R, block)
        st1[i] = stc[...].T[0:8, :]
        for k in (1, 2, 3):
            st1_send(i, k).start()

    loop(TILES, filter_tile)

    for copy in late:
        copy.wait()

    def mixed(i):
        rows = pl.ds(pl.multiple_of(i * T, T), T)
        out = rows_product(g[rows, :], wp[...])
        for h in range(2):
            gm[h, rows, :] = out[:, h * 128 : h * 128 + 128]

    loop(TILES, mixed)

    def activate(i):
        for k in (1, 2, 3):
            st1_send(i, k).wait_recv()
        sums = st1[i] + got1[i, 0] + got1[i, 1] + got1[i, 2]
        mean = sums[0:1] / CH
        var = sums[1:2] / CH - mean * mean
        wide[0:1, :] = mean
        wide[1:2, :] = lax.rsqrt(var + EPS)
        col_a[i] = wide[...].T

        def block(b):
            local_rows = pl.ds(pl.multiple_of(b * R, R), R)
            rows = pl.ds(pl.multiple_of(i * T + b * R, R), R)
            mean = col_a[i, local_rows, 0:1]
            inv = col_a[i, local_rows, 1:2]
            first, second = 0.0, 0.0
            for h in range(2):
                lanes = slice(h * 128, h * 128 + 128)
                normed = (filt[h, rows, :] - mean) * inv
                act = normed * gain[0:1, lanes] + shift[0:1, lanes]
                sig = jax.nn.sigmoid(act)
                mx[rows, lanes] = (act * sig).astype(BF)
                grad = gm[h, rows, :] * sig * (1.0 + act * (1.0 - sig))
                gs[0, h] = gs[0, h] + (grad * normed).reshape(R // 8, 8, 128).sum(axis=0)
                gs[1, h] = gs[1, h] + grad.reshape(R // 8, 8, 128).sum(axis=0)
                grad = grad * gain[0:1, lanes]
                filt[h, rows, :] = normed
                gm[h, rows, :] = grad
                first = first + grad
                second = second + grad * normed
            first = jnp.sum(first, axis=1, keepdims=True)
            second = jnp.sum(second, axis=1, keepdims=True)
            stc[local_rows, :] = jnp.where(lane == 0, first, jnp.where(lane == 1, second, 0.0))

        loop(T // R, block)
        st2[i] = stc[...].T[0:8, :]
        for k in (1, 2, 3):
            st2_send(i, k).start()

    loop(TILES, activate)

    def pair_send(n):
        return remote(wbuf.at[n, :, 1 - c], got_w.at[n], ws.at[n], wr.at[n], partner)

    def y_send(n, k):
        return remote(
            s1.at[n, :, (y + k) % 4], got_y.at[n, k - 1], ys.at[n, k - 1], yr.at[n, k - 1], at_y(k)
        )

    def z_send(n, k):
        return remote(
            s2.at[n, (z + k) % 8], got_z.at[n, k - 1], zs.at[n, k - 1], zr.at[n, k - 1], at_z(k)
        )

    def weight_chunk(n):
        source, other, off = (g, mx, 0) if n == 0 else (x, gb, (n - 1) * 256)

        def tile(zb):
            span = pl.ds(pl.multiple_of(zb * 256, 256), 256)
            out = cols_product(source[:, span], other[:, off : off + 256])
            wbuf[n, pl.ds(zb * 4, 4)] = out.astype(BF).reshape(4, 2, 32, 256)

        loop(8, tile)
        pair_send(n).start()

    def pair_sum(n):
        pair_send(n).wait_recv()

        def tile(zb):
            rows = pl.ds(zb * 4, 4)
            s1[n, zb] = (wbuf[n, rows, c].astype(F32) + got_w[n, rows].astype(F32)).astype(BF)

        loop(8, tile)
        for k in (1, 2, 3):
            y_send(n, k).start()

    def y_sum(n):
        for k in (1, 2, 3):
            y_send(n, k).wait_recv()
        total = s1[n, :, y].astype(F32)
        for k in range(3):
            total = total + got_y[n, k].astype(F32)
        s2[n] = total.astype(BF)
        for k in range(1, 8):
            z_send(n, k).start()

    def z_sum(n):
        for k in range(1, 8):
            z_send(n, k).wait_recv()
        total = s2[n, z].astype(F32)
        for k in range(7):
            total = total + got_z[n, k].astype(F32)
        w_out[n] = total * scale

    weight_chunk(0)

    def filtered_grad(i):
        for k in (1, 2, 3):
            st2_send(i, k).wait_recv()
        sums = (st2[i] + got2[i, 0] + got2[i, 1] + got2[i, 2]) / CH
        wide[0:2, :] = sums[0:2]
        col_b[...] = wide[...].T

        def block(b):
            local_rows = pl.ds(pl.multiple_of(b * R, R), R)
            rows = pl.ds(pl.multiple_of(i * T + b * R, R), R)
            inv = col_a[i, local_rows, 1:2]
            m1 = col_b[local_rows, 0:1]
            m2 = col_b[local_rows, 1:2]
            for h in range(2):
                gf[h, rows, :] = inv * (gm[h, rows, :] - m1 - filt[h, rows, :] * m2)

        loop(T // R, block)

    filtered_grad(0)
    grad_send.start()
    loop(TILES - 1, lambda i: filtered_grad(i + 1))
    pair_sum(0)
    grad_send.wait_recv()
    gf[:, 1024:1056, :] = jnp.where(s == last_sp, 0.0, gf_halo[...])

    def toward(i):
        first = i < TILES // 2
        return jnp.where(first, right, left), jnp.where(first, left, right)

    def a_send(i):
        return remote(part.at[0, i], got_a.at[i], as_.at[i], ar.at[i], {"tp": toward(i)[0]})

    def b_send(i):
        return remote(part.at[1, i], got_b.at[i], bs.at[i], br.at[i], {"tp": toward(i)[1]})

    def c_send(i):
        return remote(part.at[2, i], got_c.at[i], cs.at[i], cr.at[i], {"tp": toward(i)[0]})

    def back_tile(i):
        for h in range(2):
            lanes = slice(h * 128, h * 128 + 128)
            lanes_g = slice(256 + h * 128, 384 + h * 128)

            def block(b, h=h, lanes=lanes, lanes_g=lanes_g):
                base = pl.multiple_of(i * T + b * R, R)
                rows = pl.ds(base, R)
                gated = gi[h, pl.ds(pl.multiple_of(base + 32, 32), R), :]
                acc = jnp.zeros((R, 128), F32)
                for k in range(TAPS):
                    moved = gf[h, pl.ds(base + k, R), :]
                    acc = acc + taps[k : k + 1, lanes] * moved
                    tg[h, k] = tg[h, k] + (gated * moved).reshape(R // 8, 8, 128).sum(axis=0)
                sig = sg[h, rows, :]
                gv = acc * sig
                gb[rows, lanes] = gv.astype(BF)
                gb[rows, lanes_g] = (gv * vf[h, rows, :] * (1.0 - sig)).astype(BF)

            loop(T // R, block)

        rows = pl.ds(pl.multiple_of(i * T, T), T)

        def partial(block):
            span = pl.ds(pl.multiple_of(block * 512, 512), 512)
            return rows_product(gb[rows, 0:256], wv[span, :]) + rows_product(
                gb[rows, 256:512], wg[span, :]
            )

        near, back = toward(i)
        part[0, i] = partial(far).astype(BF)
        a_send(i).start()
        part[1, i] = partial(back).astype(BF)
        b_send(i).start()
        part[2, i] = partial(near).astype(BF)
        own[i] = partial(t)

    loop(TILES, back_tile)

    def combine(i):
        a_send(i).wait_recv()
        part[2, i] = (part[2, i].astype(F32) + got_a[i].astype(F32)).astype(BF)
        c_send(i).start()

    for h in range(2):
        lanes = slice(h * 128, h * 128 + 128)
        smb[0, 0:TAPS, lanes] = jnp.sum(tg[h], axis=1)
        smb[0, 31:32, lanes] = jnp.sum(gs[0, h], axis=0, keepdims=True)
        smb[0, 32:33, lanes] = jnp.sum(gs[1, h], axis=0, keepdims=True)
    smb[0, 33:40, :] = jnp.zeros((7, 256), F32)
    sm_pair = remote(smb.at[0], sm_c, ms.at[0], mr.at[0], partner)
    sm_pair.start()

    combine(0)
    weight_chunk(1)
    y_sum(0)
    sm_pair.wait_recv()
    smb[1] = smb[0] + sm_c[...]
    sm_ys = [remote(smb.at[1], sm_y.at[k - 1], ms.at[k], mr.at[k], at_y(k)) for k in (1, 2, 3)]
    for copy in sm_ys:
        copy.start()
    pair_sum(1)
    combine(1)
    weight_chunk(2)
    pair_sum(2)
    for copy in sm_ys:
        copy.wait_recv()
    smb[2] = smb[1] + sm_y[0] + sm_y[1] + sm_y[2]
    sm_zs = [
        remote(smb.at[2], sm_z.at[k - 1], ms.at[3 + k], mr.at[3 + k], at_z(k)) for k in range(1, 8)
    ]
    for copy in sm_zs:
        copy.start()
    y_sum(1)
    y_sum(2)
    combine(2)
    combine(3)
    z_sum(0)
    for copy in sm_zs:
        copy.wait_recv()
    total = smb[2]
    for k in range(7):
        total = total + sm_z[k]
    sm_out[...] = total * scale
    z_sum(1)
    z_sum(2)

    def finish(i):
        b_send(i).wait_recv()
        c_send(i).wait_recv()
        rows = pl.ds(pl.multiple_of(i * T, T), T)
        ig_out[rows, :] = (own[i] + got_b[i].astype(F32) + got_c[i].astype(F32)).astype(BF)

    loop(TILES, finish)

    halo_send.wait_send()
    grad_send.wait_send()
    for copy in [sm_pair, *sm_ys, *sm_zs]:
        copy.wait_send()
    for n in range(3):
        pair_send(n).wait_send()
        for k in (1, 2, 3):
            y_send(n, k).wait_send()
        for k in range(1, 8):
            z_send(n, k).wait_send()

    def drain(i):
        for k in (1, 2, 3):
            st1_send(i, k).wait_send()
            st2_send(i, k).wait_send()
        a_send(i).wait_send()
        b_send(i).wait_send()
        c_send(i).wait_send()

    loop(TILES, drain)


def module(scale, x, g, wv, wg, taps, gain, shift, wp):
    dma = pltpu.SemaphoreType.DMA
    vmem = pl.BlockSpec(memory_space=pltpu.VMEM)
    hbm = pl.BlockSpec(memory_space=pl.ANY)

    def half(rows, kind=F32):
        return pltpu.VMEM((2, rows, 128), kind)

    tile = pltpu.VMEM((TILES, T, 512), BF)
    return pl.pallas_call(
        functools.partial(whole, scale),
        out_shape=(
            jax.ShapeDtypeStruct((1024, 512), BF),
            jax.ShapeDtypeStruct((3, 32, 256), F32),
            jax.ShapeDtypeStruct((40, 256), F32),
        ),
        in_specs=[hbm, hbm, hbm, hbm, vmem, vmem, vmem, hbm],
        out_specs=(vmem,) * 3,
        scratch_shapes=[
            pltpu.VMEM((1024, 2048), BF), pltpu.VMEM((1024, 2048), BF),
            pltpu.VMEM((2048, 256), BF), pltpu.VMEM((2048, 256), BF), pltpu.VMEM((256, 2048), BF),
            dma((8,)),
            half(1056), half(32), half(1024), half(1024), half(1024), half(1024), half(1056), half(32),
            pltpu.VMEM((1024, 512), BF), pltpu.VMEM((1024, 256), BF),
            pltpu.VMEM((2, TAPS, 8, 128), F32), pltpu.VMEM((2, 2, 8, 128), F32),
            pltpu.VMEM((T, 128), F32), pltpu.VMEM((128, T), F32),
            pltpu.VMEM((TILES, T, 128), F32), pltpu.VMEM((T, 128), F32),
            pltpu.VMEM((TILES, 8, T), F32), pltpu.VMEM((TILES, 3, 8, T), F32),
            pltpu.VMEM((TILES, 8, T), F32), pltpu.VMEM((TILES, 3, 8, T), F32),
            pltpu.VMEM((3, TILES, T, 512), BF), pltpu.VMEM((TILES, T, 512), F32),
            tile, tile, tile,
            pltpu.VMEM((3, 32, 2, 32, 256), BF), pltpu.VMEM((3, 32, 32, 256), BF),
            pltpu.VMEM((3, 8, 4, 32, 256), BF), pltpu.VMEM((3, 3, 8, 32, 256), BF),
            pltpu.VMEM((3, 8, 32, 256), BF), pltpu.VMEM((3, 7, 32, 256), BF),
            pltpu.VMEM((3, 40, 256), F32), pltpu.VMEM((40, 256), F32),
            pltpu.VMEM((3, 40, 256), F32), pltpu.VMEM((7, 40, 256), F32),
            dma((2,)), dma((2,)),
            dma((TILES, 3)), dma((TILES, 3)), dma((TILES, 3)), dma((TILES, 3)),
            dma((TILES,)), dma((TILES,)), dma((TILES,)), dma((TILES,)), dma((TILES,)), dma((TILES,)),
            dma((3,)), dma((3,)), dma((3, 3)), dma((3, 3)), dma((3, 7)), dma((3, 7)),
            dma((11,)), dma((11,)),
        ],
        compiler_params=pltpu.CompilerParams(
            collective_id=0, has_side_effects=True, vmem_limit_bytes=62 * 1024 * 1024
        ),
        cost_estimate=pl.CostEstimate(
            flops=10_000_000_000, bytes_accessed=14_000_000, transcendentals=1_000_000
        ),
    )(x, g, wv, wg, taps, gain, shift, wp)


def placed(ig, w, sm, ig_out, v_out, g_out, p_out, t_out, gain_out, shift_out):
    ig_out[...] = ig[...]
    v_out[...] = w[1]
    g_out[...] = w[2]
    p_out[...] = w[0].T
    t_out[...] = sm[0:TAPS]
    gain_out[...] = sm[TAPS : TAPS + 1]
    shift_out[...] = sm[TAPS + 1 : TAPS + 2]


def shards(block_input, out_grad, w_value, w_gate, conv_taps, norm_gain, norm_shift, w_proj):
    loss_scale = 1.0 / math.sqrt(block_input.shape[0] * lax.axis_size(SP))
    parts = module(
        loss_scale, block_input, out_grad, w_value, w_gate, conv_taps,
        norm_gain.reshape(1, -1), norm_shift.reshape(1, -1), w_proj,
    )
    shapes = [
        ((1024, 512), BF), ((32, 256), F32), ((32, 256), F32), ((256, 32), F32),
        ((TAPS, 256), F32), ((1, 256), F32), ((1, 256), F32),
    ]
    out = pl.pallas_call(
        placed,
        out_shape=tuple(jax.ShapeDtypeStruct(*shape) for shape in shapes),
        cost_estimate=pl.CostEstimate(flops=1_000_000, bytes_accessed=2_000_000, transcendentals=0),
    )(*parts)
    return (*out[:5], out[5].reshape(-1), out[6].reshape(-1))


def solution(mesh):
    return jax.shard_map(
        shards,
        mesh=mesh,
        in_specs=(
            P(SP, None),
            P(SP, None),
            P(None, "tp"),
            P(None, "tp"),
            P(None, "tp"),
            P("tp"),
            P("tp"),
            P("tp", None),
        ),
        out_specs=(
            P(SP, "tp"),
            P(SP, "tp"),
            P(SP, "tp"),
            P("tp", SP),
            P(None, "tp"),
            P("tp"),
            P("tp"),
        ),
        check_vma=False,
    )
```

time: 217 us -> 78.7 us (0.36)
  waiting for transfers between devices: 103 us -> 0 us
  Pallas kernels: 0 us -> 76 us
  starting transfers between devices: 28.9 us -> 0 us
  other arithmetic: 25.2 us -> 0 us
  matrix products: 19.3 us -> 0 us
  blocking collectives: 14.8 us -> 0 us
  between operations: 14.2 us -> 0.64 us
  local copies, waits for them, and re-layouts: 11.5 us -> 1.59 us
    all_to_all x2 -> x0, waiting for transfers between devices: 89.8 us -> none  [the longest x1 45.8 us: sum_at_owner(): lax.all_to_all(pieces, axis, split_axis=0, concat_axis=0, tiled=True)]
    pallas_call x0 -> x2, Pallas kernels: none -> 76 us  [the longest x1 73.6 us: module(): pl.pallas_call(functools.partial(whole, scale), out_shape=(jax.ShapeDtype...]
    all_to_all x2 -> x0, starting transfers between devices: 20.7 us -> none  [the longest x1 15.8 us: sent_to_all(): lax.all_to_all(jnp.broadcast_to(x[None], (length, *x.shape)), axis, 0, 0,...]
    dot_general x7 -> x0, matrix products: 19.3 us -> none  [the longest x3 9.24 us: right_product(): lax.dot_general(left, right, (((1,), (1,)), ((), ())), preferred_element_...]
    reduce_sum x7 -> x0, other arithmetic: 16.2 us -> none  [the longest x2 6.2 us: shards(): jnp.sum(grad_filtered * extended[begin:begin + tok_rows], axis=0)]
    all_to_all x2 -> x0, blocking collectives: 14.8 us -> none  [sent_to_all(): lax.all_to_all(jnp.broadcast_to(x[None], (length, *x.shape)), axis, 0, 0,...]
    unnamed x5 -> x0, waiting for transfers between devices: 8.47 us -> none
    ppermute x2 -> x0, starting transfers between devices: 7.87 us -> none  [from_behind(): return lax.ppermute(block, axis, route)]
  transfers between devices with their start and end apart: 7 -> 0, of which waited for: 6 -> 0; matrix products, arithmetic and copies ran while one was open for 10% -> 0% of each run, Pallas kernels for 0% -> 0%
where the time goes in v2:
time: 78.7 us; the launch traced here: 78.2 us
  Pallas kernels  76 us (97%)
  local copies, waits for them, and re-layouts  1.59 us (2%)
    pallas_call x1, Pallas kernels, module(): pl.pallas_call(functools.partial(whole, scale), out_shape=(jax.ShapeDtype...  73.6 us
    pallas_call x1, Pallas kernels, shards(): pl.pallas_call(placed, out_shape=tuple((jax.ShapeDtypeStruct(*shape) for...  2.38 us
    unnamed x1, local copies, waits for them, and re-layouts  1.59 us

profile of v2, /device:TPU:1, one launch (start us, length us, event | category | flops | bytes accessed | tf_op | source)
XLA Modules:
  0.0 78.2 jit_solution(14129197025137466397)
XLA Ops:
  0.6 73.6 %shard_map.135 = (bf16[1024,512]{1,0:T(8,128)(2,1)}, f32[3,32,256]{2,1,0:T(8,128)}, f32[40,256]{1,0:T(8,128)}) custom-call(bf16[1024,2048]{1,0:T(8,128)(2,1)} %x_h.1, bf16[1024,2048]{1,0:T(8,128)(2,1)} %g_h.1, bf16[2048,256]{1,0:T(8,128)(2,1)} %wv_h.1, bf16[2048,256]{1,0:T(8,128)(2,1)} %wg_h.1, f32[31,256]{1,0:T(8,128)} %taps.1, f32[1,256]{1,0:T(1,128)} %bitcast.4, ...), custom_call_target="tpu_custom_call" | custom-call | flops 10000000000 | bytes 14000000 | tf_op jit(solution)/shard_map/pallas_call | solution.py:435
  74.2 2.4 %shard_map.136 = (bf16[1024,512]{1,0:T(8,128)(2,1)}, f32[32,256]{1,0:T(8,128)}, f32[32,256]{1,0:T(8,128)}, f32[256,32]{1,0:T(8,128)}, f32[31,256]{1,0:T(8,128)}, /*index=5*/f32[1,256]{1,0:T(1,128)}, f32[1,256]{1,0:T(1,128)}) custom-call(bf16[1024,512]{1,0:T(8,128)(2,1)} %get-tuple-element.17.ig, f32[3,32,256]{2,1,0:T(8,128)} %get-tuple-element.18.w, ...), custom_call_target="tpu_custom_call" | custom-call | flops 1000000 | bytes 2000000 | tf_op jit(solution)/shard_map/pallas_call | solution.py:497
  76.6 1.6 %copy.15 = f32[256,32]{0,1:T(8,128)} copy(f32[256,32]{1,0:T(8,128)} %get-tuple-element.30) | data formatting | bytes 65536

commit v3 on v2

--- a/solution.py
+++ b/solution.py
@@ -32,6 +32,10 @@
     return lax.dot_general(left, right, (((0,), (0,)), ((), ())), preferred_element_type=F32)
 
 
+def logistic(v):
+    return 0.5 * jnp.tanh(0.5 * v) + 0.5
+
+
 def loop(count, body):
     def step(i, carry):
         body(i)
@@ -46,7 +50,7 @@
     ig_out, w_out, sm_out,
     x, g, wv, wg, wp, load,
     gi, gi_halo, vf, sg, filt, gm, gf, gf_halo, gb, mx, tg, gs,
-    stc, wide, col_a, col_b, st1, got1, st2, got2,
+    sum_a, sum_b, col_m, col_i, col_a, col_b, st1, got1, st2, got2,
     part, own, got_a, got_b, got_c,
     wbuf, got_w, s1, got_y, s2, got_z,
     smb, sm_c, sm_y, sm_z,
@@ -100,10 +104,17 @@
             device_id=device, device_id_type=MESH,
         )
 
-    lane = lax.broadcasted_iota(jnp.int32, (R, 128), 1)
     tg[...] = jnp.zeros_like(tg)
     gs[...] = jnp.zeros_like(gs)
-    wide[...] = jnp.zeros_like(wide)
+    st1[...] = jnp.zeros_like(st1)
+    st2[...] = jnp.zeros_like(st2)
+
+    def token_sums(tile):
+        return jnp.sum(tile[...].T, axis=0, keepdims=True)
+
+    def over_lanes(row):
+        return jnp.broadcast_to(row, (128, T)).T
+
 
     halo_send = remote(gi.at[:, pl.ds(1024, 32)], gi_halo, hs.at[0], hr.at[0], after)
     grad_send = remote(gf.at[:, pl.ds(0, 32)], gf_halo, hs.at[1], hr.at[1], before)
@@ -119,7 +130,7 @@
         x_rows(i).wait()
         value = plain(x[rows, :], wv[...]).astype(BF).astype(F32)
         gate = plain(x[rows, :], wg[...]).astype(BF).astype(F32)
-        sig = jax.nn.sigmoid(gate)
+        sig = logistic(gate)
         gated = (value * sig).astype(BF).astype(F32)
         at = pl.ds(pl.multiple_of(i * T + 32, 32), T)
         for h in range(2):
@@ -128,41 +139,29 @@
             sg[h, rows, :] = sig[:, lanes]
             gi[h, at, :] = gated[:, lanes]
 
-    for copy in loads:
-        copy.wait()
-    project(3)
-    pl.semaphore_wait(barrier, len(peers))
-    halo_send.start()
-    loop(3, project)
-    halo_send.wait_recv()
-    gi[:, 0:32, :] = jnp.where(s == 0, 0.0, gi_halo[...])
-
     def filter_tile(i):
         def block(b):
-            base = pl.multiple_of(i * T + b * R, R)
-            out = []
+            base = pl.multiple_of(i * T + b * 128, 128)
+            rows = pl.ds(base, 128)
+            tile = pl.ds(pl.multiple_of(b * 128, 128), 128)
             for h in range(2):
-                acc = jnp.zeros((R, 128), F32)
+                acc = jnp.zeros((128, 128), F32)
                 for k in range(TAPS):
                     tap = taps[k : k + 1, h * 128 : h * 128 + 128]
-                    acc = acc + tap * gi[h, pl.ds(base + 32 - k, R), :]
-                filt[h, pl.ds(base, R), :] = acc
-                out.append(acc)
-            total = jnp.sum(out[0] + out[1], axis=1, keepdims=True)
-            square = jnp.sum(out[0] * out[0] + out[1] * out[1], axis=1, keepdims=True)
-            stc[pl.ds(pl.multiple_of(b * R, R), R), :] = jnp.where(
-                lane == 0, total, jnp.where(lane == 1, square, 0.0)
-            )
-
-        loop(T // R, block)
-        st1[i] = stc[...].T[0:8, :]
+                    acc = acc + tap * gi[h, pl.ds(base + 32 - k, 128), :]
+                filt[h, rows, :] = acc
+                if h == 0:
+                    sum_a[tile, :] = acc
+                    sum_b[tile, :] = acc * acc
+                else:
+                    sum_a[tile, :] = sum_a[tile, :] + acc
+                    sum_b[tile, :] = sum_b[tile, :] + acc * acc
+
+        loop(T // 128, block)
+        st1[i, 0:1] = token_sums(sum_a)
+        st1[i, 1:2] = token_sums(sum_b)
         for k in (1, 2, 3):
             st1_send(i, k).start()
-
-    loop(TILES, filter_tile)
-
-    for copy in late:
-        copy.wait()
 
     def mixed(i):
         rows = pl.ds(pl.multiple_of(i * T, T), T)
@@ -170,29 +169,26 @@
         for h in range(2):
             gm[h, rows, :] = out[:, h * 128 : h * 128 + 128]
 
-    loop(TILES, mixed)
-
     def activate(i):
         for k in (1, 2, 3):
             st1_send(i, k).wait_recv()
         sums = st1[i] + got1[i, 0] + got1[i, 1] + got1[i, 2]
         mean = sums[0:1] / CH
         var = sums[1:2] / CH - mean * mean
-        wide[0:1, :] = mean
-        wide[1:2, :] = lax.rsqrt(var + EPS)
-        col_a[i] = wide[...].T
+        col_m[i] = over_lanes(mean)
+        col_i[i] = over_lanes(lax.rsqrt(var + EPS))
 
         def block(b):
             local_rows = pl.ds(pl.multiple_of(b * R, R), R)
             rows = pl.ds(pl.multiple_of(i * T + b * R, R), R)
-            mean = col_a[i, local_rows, 0:1]
-            inv = col_a[i, local_rows, 1:2]
+            mean = col_m[i, local_rows, :]
+            inv = col_i[i, local_rows, :]
             first, second = 0.0, 0.0
             for h in range(2):
                 lanes = slice(h * 128, h * 128 + 128)
                 normed = (filt[h, rows, :] - mean) * inv
                 act = normed * gain[0:1, lanes] + shift[0:1, lanes]
-                sig = jax.nn.sigmoid(act)
+                sig = logistic(act)
                 mx[rows, lanes] = (act * sig).astype(BF)
                 grad = gm[h, rows, :] * sig * (1.0 + act * (1.0 - sig))
                 gs[0, h] = gs[0, h] + (grad * normed).reshape(R // 8, 8, 128).sum(axis=0)
@@ -202,16 +198,14 @@
                 gm[h, rows, :] = grad
                 first = first + grad
                 second = second + grad * normed
-            first = jnp.sum(first, axis=1, keepdims=True)
-            second = jnp.sum(second, axis=1, keepdims=True)
-            stc[local_rows, :] = jnp.where(lane == 0, first, jnp.where(lane == 1, second, 0.0))
+            sum_a[local_rows, :] = first
+            sum_b[local_rows, :] = second
 
         loop(T // R, block)
-        st2[i] = stc[...].T[0:8, :]
+        st2[i, 0:1] = token_sums(sum_a)
+        st2[i, 1:2] = token_sums(sum_b)
         for k in (1, 2, 3):
             st2_send(i, k).start()
-
-    loop(TILES, activate)
 
     def pair_send(n):
         return remote(wbuf.at[n, :, 1 - c], got_w.at[n], ws.at[n], wr.at[n], partner)
@@ -226,16 +220,25 @@
             s2.at[n, (z + k) % 8], got_z.at[n, k - 1], zs.at[n, k - 1], zr.at[n, k - 1], at_z(k)
         )
 
-    def weight_chunk(n):
-        source, other, off = (g, mx, 0) if n == 0 else (x, gb, (n - 1) * 256)
-
+    def proj_chunk():
         def tile(zb):
-            span = pl.ds(pl.multiple_of(zb * 256, 256), 256)
-            out = cols_product(source[:, span], other[:, off : off + 256])
-            wbuf[n, pl.ds(zb * 4, 4)] = out.astype(BF).reshape(4, 2, 32, 256)
-
-        loop(8, tile)
-        pair_send(n).start()
+            span = pl.ds(pl.multiple_of(zb * 512, 512), 512)
+            out = cols_product(g[:, span], mx[...]).astype(BF)
+            wbuf[0, pl.ds(zb * 8, 8)] = out.reshape(8, 2, 32, 256)
+
+        loop(4, tile)
+        pair_send(0).start()
+
+    def gate_chunks():
+        def tile(zb):
+            span = pl.ds(pl.multiple_of(zb * 512, 512), 512)
+            out = cols_product(x[:, span], gb[...]).astype(BF)
+            for n in (0, 1):
+                wbuf[n + 1, pl.ds(zb * 8, 8)] = out[:, n * 256 : n * 256 + 256].reshape(8, 2, 32, 256)
+
+        loop(4, tile)
+        pair_send(1).start()
+        pair_send(2).start()
 
     def pair_sum(n):
         pair_send(n).wait_recv()
@@ -266,32 +269,23 @@
             total = total + got_z[n, k].astype(F32)
         w_out[n] = total * scale
 
-    weight_chunk(0)
-
     def filtered_grad(i):
         for k in (1, 2, 3):
             st2_send(i, k).wait_recv()
         sums = (st2[i] + got2[i, 0] + got2[i, 1] + got2[i, 2]) / CH
-        wide[0:2, :] = sums[0:2]
-        col_b[...] = wide[...].T
+        col_a[...] = over_lanes(sums[0:1])
+        col_b[...] = over_lanes(sums[1:2])
 
         def block(b):
             local_rows = pl.ds(pl.multiple_of(b * R, R), R)
             rows = pl.ds(pl.multiple_of(i * T + b * R, R), R)
-            inv = col_a[i, local_rows, 1:2]
-            m1 = col_b[local_rows, 0:1]
-            m2 = col_b[local_rows, 1:2]
+            inv = col_i[i, local_rows, :]
+            m1 = col_a[local_rows, :]
+            m2 = col_b[local_rows, :]
             for h in range(2):
                 gf[h, rows, :] = inv * (gm[h, rows, :] - m1 - filt[h, rows, :] * m2)
 
         loop(T // R, block)
-
-    filtered_grad(0)
-    grad_send.start()
-    loop(TILES - 1, lambda i: filtered_grad(i + 1))
-    pair_sum(0)
-    grad_send.wait_recv()
-    gf[:, 1024:1056, :] = jnp.where(s == last_sp, 0.0, gf_halo[...])
 
     def toward(i):
         first = i < TILES // 2
@@ -343,12 +337,53 @@
         part[2, i] = partial(near).astype(BF)
         own[i] = partial(t)
 
-    loop(TILES, back_tile)
-
     def combine(i):
         a_send(i).wait_recv()
         part[2, i] = (part[2, i].astype(F32) + got_a[i].astype(F32)).astype(BF)
         c_send(i).start()
+
+    def pair(first, body):
+        loop(2, lambda j: body(first + j))
+
+    for copy in loads:
+        copy.wait()
+    project(3)
+    pl.semaphore_wait(barrier, len(peers))
+    halo_send.start()
+    pair(0, project)
+    halo_send.wait_recv()
+    gi[:, 0:32, :] = jnp.where(s == 0, 0.0, gi_halo[...])
+    pair(0, filter_tile)
+    project(2)
+    for copy in late:
+        copy.wait()
+    pair(0, mixed)
+    pair(0, activate)
+    pair(2, filter_tile)
+    filtered_grad(0)
+    grad_send.start()
+    filtered_grad(1)
+    back_tile(0)
+    pair(2, mixed)
+    pair(2, activate)
+
+    def middle(j):
+        @pl.when(j == 2)
+        def _():
+            proj_chunk()
+
+        @pl.when(j < 3)
+        def _():
+            filtered_grad(j + 1)
+
+        @pl.when(j == 3)
+        def _():
+            grad_send.wait_recv()
+            gf[:, 1024:1056, :] = jnp.where(s == last_sp, 0.0, gf_halo[...])
+
+        back_tile(j)
+
+    loop(3, lambda j: middle(j + 1))
 
     for h in range(2):
         lanes = slice(h * 128, h * 128 + 128)
@@ -358,19 +393,16 @@
     smb[0, 33:40, :] = jnp.zeros((7, 256), F32)
     sm_pair = remote(smb.at[0], sm_c, ms.at[0], mr.at[0], partner)
     sm_pair.start()
-
-    combine(0)
-    weight_chunk(1)
-    y_sum(0)
+    pair_sum(0)
+    gate_chunks()
     sm_pair.wait_recv()
     smb[1] = smb[0] + sm_c[...]
     sm_ys = [remote(smb.at[1], sm_y.at[k - 1], ms.at[k], mr.at[k], at_y(k)) for k in (1, 2, 3)]
     for copy in sm_ys:
         copy.start()
-    pair_sum(1)
-    combine(1)
-    weight_chunk(2)
-    pair_sum(2)
+    loop(2, lambda j: pair_sum(j + 1))
+    pair(0, combine)
+    y_sum(0)
     for copy in sm_ys:
         copy.wait_recv()
     smb[2] = smb[1] + sm_y[0] + sm_y[1] + sm_y[2]
@@ -379,10 +411,8 @@
     ]
     for copy in sm_zs:
         copy.start()
-    y_sum(1)
-    y_sum(2)
-    combine(2)
-    combine(3)
+    loop(2, lambda j: y_sum(j + 1))
+    pair(2, combine)
     z_sum(0)
     for copy in sm_zs:
         copy.wait_recv()
@@ -390,8 +420,7 @@
     for k in range(7):
         total = total + sm_z[k]
     sm_out[...] = total * scale
-    z_sum(1)
-    z_sum(2)
+    loop(2, lambda j: z_sum(j + 1))
 
     def finish(i):
         b_send(i).wait_recv()
@@ -448,8 +477,9 @@
             half(1056), half(32), half(1024), half(1024), half(1024), half(1024), half(1056), half(32),
             pltpu.VMEM((1024, 512), BF), pltpu.VMEM((1024, 256), BF),
             pltpu.VMEM((2, TAPS, 8, 128), F32), pltpu.VMEM((2, 2, 8, 128), F32),
-            pltpu.VMEM((T, 128), F32), pltpu.VMEM((128, T), F32),
-            pltpu.VMEM((TILES, T, 128), F32), pltpu.VMEM((T, 128), F32),
+            pltpu.VMEM((T, 128), F32), pltpu.VMEM((T, 128), F32),
+            pltpu.VMEM((TILES, T, 128), F32), pltpu.VMEM((TILES, T, 128), F32),
+            pltpu.VMEM((T, 128), F32), pltpu.VMEM((T, 128), F32),
             pltpu.VMEM((TILES, 8, T), F32), pltpu.VMEM((TILES, 3, 8, T), F32),
             pltpu.VMEM((TILES, 8, T), F32), pltpu.VMEM((TILES, 3, 8, T), F32),
             pltpu.VMEM((3, TILES, T, 512), BF), pltpu.VMEM((TILES, T, 512), F32),
@@ -478,7 +508,7 @@
     ig_out[...] = ig[...]
     v_out[...] = w[1]
     g_out[...] = w[2]
-    p_out[...] = w[0].T
+    p_out[...] = w[0]
     t_out[...] = sm[0:TAPS]
     gain_out[...] = sm[TAPS : TAPS + 1]
     shift_out[...] = sm[TAPS + 1 : TAPS + 2]
@@ -491,7 +521,7 @@
         norm_gain.reshape(1, -1), norm_shift.reshape(1, -1), w_proj,
     )
     shapes = [
-        ((1024, 512), BF), ((32, 256), F32), ((32, 256), F32), ((256, 32), F32),
+        ((1024, 512), BF), ((32, 256), F32), ((32, 256), F32), ((32, 256), F32),
         ((TAPS, 256), F32), ((1, 256), F32), ((1, 256), F32),
     ]
     out = pl.pallas_call(
@@ -499,7 +529,7 @@
         out_shape=tuple(jax.ShapeDtypeStruct(*shape) for shape in shapes),
         cost_estimate=pl.CostEstimate(flops=1_000_000, bytes_accessed=2_000_000, transcendentals=0),
     )(*parts)
-    return (*out[:5], out[5].reshape(-1), out[6].reshape(-1))
+    return (*out[:3], out[3].T, out[4], out[5].reshape(-1), out[6].reshape(-1))
 
 
 def solution(mesh):

time: 78.7 us -> 78.3 us (level)
  local copies, waits for them, and re-layouts: 1.59 us -> 0 us
  Pallas kernels: 76 us -> 76.8 us
    unnamed x1 -> x0, local copies, waits for them, and re-layouts: 1.59 us -> none
    pallas_call x1, Pallas kernels: 73.6 us -> 74.5 us  [module(): pl.pallas_call(functools.partial(whole, scale), out_shape=(jax.ShapeDtype...]
where the time goes in v3:
time: 78.3 us; the launch traced here: 77.5 us
  Pallas kernels  76.8 us (98%)
    pallas_call x1, Pallas kernels, module(): pl.pallas_call(functools.partial(whole, scale), out_shape=(jax.ShapeDtype...  74.5 us
    pallas_call x1, Pallas kernels, shards(): pl.pallas_call(placed, out_shape=tuple((jax.ShapeDtypeStruct(*shape) for...  2.34 us

profile of v3, /device:TPU:1, one launch (start us, length us, event | category | flops | bytes accessed | tf_op | source)
XLA Modules:
  0.0 77.5 jit_solution(5316062580837303384)
XLA Ops:
  0.6 74.5 %shard_map.135 = (bf16[1024,512]{1,0:T(8,128)(2,1)}, f32[3,32,256]{2,1,0:T(8,128)}, f32[40,256]{1,0:T(8,128)}) custom-call(bf16[1024,2048]{1,0:T(8,128)(2,1)} %x_h.1, bf16[1024,2048]{1,0:T(8,128)(2,1)} %g_h.1, bf16[2048,256]{1,0:T(8,128)(2,1)} %wv_h.1, bf16[2048,256]{1,0:T(8,128)(2,1)} %wg_h.1, f32[31,256]{1,0:T(8,128)} %taps.1, f32[1,256]{1,0:T(1,128)} %bitcast.6, ...), custom_call_target="tpu_custom_call" | custom-call | flops 10000000000 | bytes 14000000 | tf_op jit(solution)/shard_map/pallas_call | solution.py:464
  75.1 2.3 %shard_map.136 = (bf16[1024,512]{1,0:T(8,128)(2,1)}, f32[32,256]{1,0:T(8,128)}, f32[32,256]{1,0:T(8,128)}, f32[32,256]{1,0:T(8,128)}, f32[31,256]{1,0:T(8,128)}, /*index=5*/f32[1,256]{1,0:T(1,128)}, f32[1,256]{1,0:T(1,128)}) custom-call(bf16[1024,512]{1,0:T(8,128)(2,1)} %get-tuple-element.17.ig, f32[3,32,256]{2,1,0:T(8,128)} %get-tuple-element.18.w, ...), custom_call_target="tpu_custom_call" | custom-call | flops 1000000 | bytes 2000000 | tf_op jit(solution)/shard_map/pallas_call | solution.py:527

commit v4 on v3

--- a/solution.py
+++ b/solution.py
@@ -207,27 +207,45 @@
         for k in (1, 2, 3):
             st2_send(i, k).start()
 
-    def pair_send(n):
-        return remote(wbuf.at[n, :, 1 - c], got_w.at[n], ws.at[n], wr.at[n], partner)
-
-    def y_send(n, k):
+    def pair_send(n, q):
+        rows = pl.ds(q * 8, 8)
         return remote(
-            s1.at[n, :, (y + k) % 4], got_y.at[n, k - 1], ys.at[n, k - 1], yr.at[n, k - 1], at_y(k)
+            wbuf.at[n, rows, 1 - c], got_w.at[n, rows], ws.at[n, q], wr.at[n, q], partner
         )
+
+    def y_way(q):
+        return jnp.where(q == 0, (y + 1) % 4, (y + 3) % 4), jnp.where(q == 0, (y + 3) % 4, (y + 1) % 4)
+
+    def y_move(kind, n, q, which, line):
+        rows = pl.ds(q * 4, 4)
+        return remote(
+            s1.at[n, rows, which], got_y.at[kind, n, rows], ys.at[kind, n, q], yr.at[kind, n, q],
+            {SP: (z * 4 + line) * 2 + c},
+        )
+
+    def ya_send(n, q):
+        return y_move(0, n, q, (y + 2) % 4, y_way(q)[0])
+
+    def yb_send(n, q):
+        return y_move(1, n, q, y_way(q)[1], y_way(q)[1])
+
+    def yc_send(n, q):
+        return y_move(2, n, q, y_way(q)[0], y_way(q)[0])
 
     def z_send(n, k):
         return remote(
             s2.at[n, (z + k) % 8], got_z.at[n, k - 1], zs.at[n, k - 1], zr.at[n, k - 1], at_z(k)
         )
 
-    def proj_chunk():
-        def tile(zb):
+    def proj_half(first):
+        def tile(j):
+            zb = first + j
             span = pl.ds(pl.multiple_of(zb * 512, 512), 512)
             out = cols_product(g[:, span], mx[...]).astype(BF)
             wbuf[0, pl.ds(zb * 8, 8)] = out.reshape(8, 2, 32, 256)
-
-        loop(4, tile)
-        pair_send(0).start()
+            pair_send(0, zb).start()
+
+        loop(2, tile)
 
     def gate_chunks():
         def tile(zb):
@@ -235,28 +253,37 @@
             out = cols_product(x[:, span], gb[...]).astype(BF)
             for n in (0, 1):
                 wbuf[n + 1, pl.ds(zb * 8, 8)] = out[:, n * 256 : n * 256 + 256].reshape(8, 2, 32, 256)
+                pair_send(n + 1, zb).start()
 
         loop(4, tile)
-        pair_send(1).start()
-        pair_send(2).start()
 
     def pair_sum(n):
-        pair_send(n).wait_recv()
-
-        def tile(zb):
-            rows = pl.ds(zb * 4, 4)
-            s1[n, zb] = (wbuf[n, rows, c].astype(F32) + got_w[n, rows].astype(F32)).astype(BF)
-
-        loop(8, tile)
-        for k in (1, 2, 3):
-            y_send(n, k).start()
+        def tile(q):
+            pair_send(n, q).wait_recv()
+            for r in range(2):
+                rows = pl.ds(q * 8 + r * 4, 4)
+                pair = wbuf[n, rows, c].astype(F32) + got_w[n, rows].astype(F32)
+                s1[n, q * 2 + r] = pair.astype(BF)
+
+        loop(4, tile)
+        for q in (0, 1):
+            ya_send(n, q).start()
+        for q in (0, 1):
+            yb_send(n, q).start()
+
+    def y_pass(n):
+        for q in (0, 1):
+            ya_send(n, q).wait_recv()
+            rows, line = pl.ds(q * 4, 4), y_way(q)[0]
+            pair = s1[n, rows, line].astype(F32) + got_y[0, n, rows].astype(F32)
+            s1[n, rows, line] = pair.astype(BF)
+            yc_send(n, q).start()
 
     def y_sum(n):
-        for k in (1, 2, 3):
-            y_send(n, k).wait_recv()
-        total = s1[n, :, y].astype(F32)
-        for k in range(3):
-            total = total + got_y[n, k].astype(F32)
+        for q in (0, 1):
+            yb_send(n, q).wait_recv()
+            yc_send(n, q).wait_recv()
+        total = s1[n, :, y].astype(F32) + got_y[1, n].astype(F32) + got_y[2, n].astype(F32)
         s2[n] = total.astype(BF)
         for k in range(1, 8):
             z_send(n, k).start()
@@ -350,31 +377,31 @@
     project(3)
     pl.semaphore_wait(barrier, len(peers))
     halo_send.start()
-    pair(0, project)
-    halo_send.wait_recv()
-    gi[:, 0:32, :] = jnp.where(s == 0, 0.0, gi_halo[...])
-    pair(0, filter_tile)
-    project(2)
+    loop(3, project)
     for copy in late:
         copy.wait()
     pair(0, mixed)
-    pair(0, activate)
-    pair(2, filter_tile)
+    halo_send.wait_recv()
+    gi[:, 0:32, :] = jnp.where(s == 0, 0.0, gi_halo[...])
+    loop(TILES, filter_tile)
+    pair(2, mixed)
+    loop(TILES, activate)
+    proj_half(0)
     filtered_grad(0)
     grad_send.start()
-    filtered_grad(1)
-    back_tile(0)
-    pair(2, mixed)
-    pair(2, activate)
 
     def middle(j):
-        @pl.when(j == 2)
-        def _():
-            proj_chunk()
-
         @pl.when(j < 3)
         def _():
             filtered_grad(j + 1)
+
+        @pl.when(j == 1)
+        def _():
+            proj_half(2)
+
+        @pl.when(j == 2)
+        def _():
+            pair_sum(0)
 
         @pl.when(j == 3)
         def _():
@@ -383,61 +410,74 @@
 
         back_tile(j)
 
-    loop(3, lambda j: middle(j + 1))
+    loop(TILES, middle)
 
     for h in range(2):
-        lanes = slice(h * 128, h * 128 + 128)
-        smb[0, 0:TAPS, lanes] = jnp.sum(tg[h], axis=1)
-        smb[0, 31:32, lanes] = jnp.sum(gs[0, h], axis=0, keepdims=True)
-        smb[0, 32:33, lanes] = jnp.sum(gs[1, h], axis=0, keepdims=True)
-    smb[0, 33:40, :] = jnp.zeros((7, 256), F32)
-    sm_pair = remote(smb.at[0], sm_c, ms.at[0], mr.at[0], partner)
+        smb[h, 0:TAPS] = jnp.sum(tg[h], axis=1)
+        smb[h, 31:32] = jnp.sum(gs[0, h], axis=0, keepdims=True)
+        smb[h, 32:33] = jnp.sum(gs[1, h], axis=0, keepdims=True)
+        smb[h, 33:40] = jnp.zeros((7, 128), F32)
+    sm_pair = remote(smb.at[1 - c], sm_c, ms.at[0], mr.at[0], partner)
     sm_pair.start()
-    pair_sum(0)
+    y_pass(0)
     gate_chunks()
     sm_pair.wait_recv()
-    smb[1] = smb[0] + sm_c[...]
-    sm_ys = [remote(smb.at[1], sm_y.at[k - 1], ms.at[k], mr.at[k], at_y(k)) for k in (1, 2, 3)]
+    smb[2] = smb[c] + sm_c[...]
+    sm_ys = [remote(smb.at[2], sm_y.at[k - 1], ms.at[k], mr.at[k], at_y(k)) for k in (1, 2, 3)]
     for copy in sm_ys:
         copy.start()
     loop(2, lambda j: pair_sum(j + 1))
-    pair(0, combine)
     y_sum(0)
+    combine(0)
     for copy in sm_ys:
         copy.wait_recv()
-    smb[2] = smb[1] + sm_y[0] + sm_y[1] + sm_y[2]
+    smb[3] = smb[2] + sm_y[0] + sm_y[1] + sm_y[2]
     sm_zs = [
-        remote(smb.at[2], sm_z.at[k - 1], ms.at[3 + k], mr.at[3 + k], at_z(k)) for k in range(1, 8)
+        remote(smb.at[3], sm_z.at[k - 1], ms.at[3 + k], mr.at[3 + k], at_z(k)) for k in range(1, 8)
     ]
     for copy in sm_zs:
         copy.start()
-    loop(2, lambda j: y_sum(j + 1))
-    pair(2, combine)
-    z_sum(0)
+    y_pass(1)
+    combine(1)
+    y_pass(2)
+    combine(2)
+    y_sum(1)
+    y_sum(2)
+    combine(3)
     for copy in sm_zs:
         copy.wait_recv()
-    total = smb[2]
+    total = smb[3]
     for k in range(7):
         total = total + sm_z[k]
-    sm_out[...] = total * scale
+    smb[4] = total * scale
+    sm_swap = remote(smb.at[4], smb.at[5], ms.at[11], mr.at[11], partner)
+    sm_swap.start()
+    z_sum(0)
+    sm_swap.wait_recv()
+    sm_out[c] = smb[4]
+    sm_out[1 - c] = smb[5]
     loop(2, lambda j: z_sum(j + 1))
 
     def finish(i):
         b_send(i).wait_recv()
         c_send(i).wait_recv()
-        rows = pl.ds(pl.multiple_of(i * T, T), T)
+        rows = pl.ds(i * T, T)
         ig_out[rows, :] = (own[i] + got_b[i].astype(F32) + got_c[i].astype(F32)).astype(BF)
 
-    loop(TILES, finish)
+    for i in (0, 2, 1, 3):
+        finish(i)
 
     halo_send.wait_send()
     grad_send.wait_send()
-    for copy in [sm_pair, *sm_ys, *sm_zs]:
+    for copy in [sm_pair, sm_swap, *sm_ys, *sm_zs]:
         copy.wait_send()
     for n in range(3):
-        pair_send(n).wait_send()
-        for k in (1, 2, 3):
-            y_send(n, k).wait_send()
+        for q in range(4):
+            pair_send(n, q).wait_send()
+        for q in (0, 1):
+            ya_send(n, q).wait_send()
+            yb_send(n, q).wait_send()
+            yc_send(n, q).wait_send()
         for k in range(1, 8):
             z_send(n, k).wait_send()
 
@@ -466,7 +506,7 @@
         out_shape=(
             jax.ShapeDtypeStruct((1024, 512), BF),
             jax.ShapeDtypeStruct((3, 32, 256), F32),
-            jax.ShapeDtypeStruct((40, 256), F32),
+            jax.ShapeDtypeStruct((2, 40, 128), F32),
         ),
         in_specs=[hbm, hbm, hbm, hbm, vmem, vmem, vmem, hbm],
         out_specs=(vmem,) * 3,
@@ -487,13 +527,13 @@
             pltpu.VMEM((3, 32, 2, 32, 256), BF), pltpu.VMEM((3, 32, 32, 256), BF),
             pltpu.VMEM((3, 8, 4, 32, 256), BF), pltpu.VMEM((3, 3, 8, 32, 256), BF),
             pltpu.VMEM((3, 8, 32, 256), BF), pltpu.VMEM((3, 7, 32, 256), BF),
-            pltpu.VMEM((3, 40, 256), F32), pltpu.VMEM((40, 256), F32),
-            pltpu.VMEM((3, 40, 256), F32), pltpu.VMEM((7, 40, 256), F32),
+            pltpu.VMEM((6, 40, 128), F32), pltpu.VMEM((40, 128), F32),
+            pltpu.VMEM((3, 40, 128), F32), pltpu.VMEM((7, 40, 128), F32),
             dma((2,)), dma((2,)),
             dma((TILES, 3)), dma((TILES, 3)), dma((TILES, 3)), dma((TILES, 3)),
             dma((TILES,)), dma((TILES,)), dma((TILES,)), dma((TILES,)), dma((TILES,)), dma((TILES,)),
-            dma((3,)), dma((3,)), dma((3, 3)), dma((3, 3)), dma((3, 7)), dma((3, 7)),
-            dma((11,)), dma((11,)),
+            dma((3, 4)), dma((3, 4)), dma((3, 3, 2)), dma((3, 3, 2)), dma((3, 7)), dma((3, 7)),
+            dma((12,)), dma((12,)),
         ],
         compiler_params=pltpu.CompilerParams(
             collective_id=0, has_side_effects=True, vmem_limit_bytes=62 * 1024 * 1024
@@ -506,12 +546,21 @@
 
 def placed(ig, w, sm, ig_out, v_out, g_out, p_out, t_out, gain_out, shift_out):
     ig_out[...] = ig[...]
-    v_out[...] = w[1]
-    g_out[...] = w[2]
-    p_out[...] = w[0]
-    t_out[...] = sm[0:TAPS]
-    gain_out[...] = sm[TAPS : TAPS + 1]
-    shift_out[...] = sm[TAPS + 1 : TAPS + 2]
+
+    @pl.when(pl.program_id(0) == 0)
+    def _():
+        v_out[...] = w[1]
+        g_out[...] = w[2]
+        p_out[...] = w[0]
+        for h in range(2):
+            lanes = slice(h * 128, h * 128 + 128)
+            t_out[:, lanes] = sm[h, 0:TAPS]
+            gain_out[:, lanes] = sm[h, TAPS : TAPS + 1]
+            shift_out[:, lanes] = sm[h, TAPS + 1 : TAPS + 2]
+
+
+def fixed(*shape):
+    return pl.BlockSpec(shape, lambda i: (0,) * len(shape))
 
 
 def shards(block_input, out_grad, w_value, w_gate, conv_taps, norm_gain, norm_shift, w_proj):
@@ -526,7 +575,11 @@
     ]
     out = pl.pallas_call(
         placed,
-        out_shape=tuple(jax.ShapeDtypeStruct(*shape) for shape in shapes),
+        grid=(2,),
+        in_specs=[pl.BlockSpec((512, 512), lambda i: (i, 0)), fixed(3, 32, 256), fixed(2, 40, 128)],
+        out_specs=[pl.BlockSpec((512, 512), lambda i: (i, 0))]
+        + [fixed(*shape) for shape, _ in shapes[1:]],
+        out_shape=[jax.ShapeDtypeStruct(*shape) for shape in shapes],
         cost_estimate=pl.CostEstimate(flops=1_000_000, bytes_accessed=2_000_000, transcendentals=0),
     )(*parts)
     return (*out[:3], out[3].T, out[4], out[5].reshape(-1), out[6].reshape(-1))

time: 78.3 us -> 64.8 us (0.83)
  Pallas kernels: 76.8 us -> 64 us
    pallas_call x1, Pallas kernels: 74.5 us -> 61.9 us  [module(): pl.pallas_call(functools.partial(whole, scale), out_shape=(jax.ShapeDtype...]
where the time goes in v4:
time: 64.8 us; the launch traced here: 64.6 us
  Pallas kernels  64 us (99%)
    pallas_call x1, Pallas kernels, module(): pl.pallas_call(functools.partial(whole, scale), out_shape=(jax.ShapeDtype...  61.9 us
    pallas_call x1, Pallas kernels, shards(): pl.pallas_call(placed, grid=(2,), in_specs=[pl.BlockSpec((512, 512), lamb...  2.13 us

profile of v4, /device:TPU:1, one launch (start us, length us, event | category | flops | bytes accessed | tf_op | source)
XLA Modules:
  0.0 64.6 jit_solution(15909583067686062074)
XLA Ops:
  0.6 61.9 %shard_map.135 = (bf16[1024,512]{1,0:T(8,128)(2,1)}, f32[3,32,256]{2,1,0:T(8,128)}, f32[2,40,128]{2,1,0:T(8,128)}) custom-call(bf16[1024,2048]{1,0:T(8,128)(2,1)} %x_h.1, bf16[1024,2048]{1,0:T(8,128)(2,1)} %g_h.1, bf16[2048,256]{1,0:T(8,128)(2,1)} %wv_h.1, bf16[2048,256]{1,0:T(8,128)(2,1)} %wg_h.1, f32[31,256]{1,0:T(8,128)} %taps.1, f32[1,256]{1,0:T(1,128)} %bitcast.6, ...), custom_call_target="tpu_custom_call" | custom-call | flops 10000000000 | bytes 14000000 | tf_op jit(solution)/shard_map/pallas_call | solution.py:504
  62.5 2.1 %shard_map.136 = (bf16[1024,512]{1,0:T(8,128)(2,1)}, f32[32,256]{1,0:T(8,128)}, f32[32,256]{1,0:T(8,128)}, f32[32,256]{1,0:T(8,128)}, f32[31,256]{1,0:T(8,128)}, /*index=5*/f32[1,256]{1,0:T(1,128)}, f32[1,256]{1,0:T(1,128)}) custom-call(bf16[1024,512]{1,0:T(8,128)(2,1)} %get-tuple-element.17.ig, f32[3,32,256]{2,1,0:T(8,128)} %get-tuple-element.18.w, ...), custom_call_target="tpu_custom_call" | custom-call | flops 1000000 | bytes 2000000 | tf_op jit(solution)/shard_map/pallas_call | solution.py:576

commit v5 on v4

--- a/solution.py
+++ b/solution.py
@@ -139,7 +139,7 @@
             sg[h, rows, :] = sig[:, lanes]
             gi[h, at, :] = gated[:, lanes]
 
-    def filter_tile(i):
+    def filter_rows(i):
         def block(b):
             base = pl.multiple_of(i * T + b * 128, 128)
             rows = pl.ds(base, 128)
@@ -160,8 +160,14 @@
         loop(T // 128, block)
         st1[i, 0:1] = token_sums(sum_a)
         st1[i, 1:2] = token_sums(sum_b)
-        for k in (1, 2, 3):
+
+    def filter_tell(i):
+        for k in (2, 1, 3):
             st1_send(i, k).start()
+
+    def filter_tile(i):
+        filter_rows(i)
+        filter_tell(i)
 
     def mixed(i):
         rows = pl.ds(pl.multiple_of(i * T, T), T)
@@ -247,36 +253,37 @@
 
         loop(2, tile)
 
-    def gate_chunks():
-        def tile(zb):
+    def gate_chunks(first, count):
+        def tile(j):
+            zb = first + j
             span = pl.ds(pl.multiple_of(zb * 512, 512), 512)
             out = cols_product(x[:, span], gb[...]).astype(BF)
             for n in (0, 1):
                 wbuf[n + 1, pl.ds(zb * 8, 8)] = out[:, n * 256 : n * 256 + 256].reshape(8, 2, 32, 256)
                 pair_send(n + 1, zb).start()
 
-        loop(4, tile)
+        loop(count, tile)
+
+    def pair_half(n, q):
+        def tile(j):
+            pair_send(n, q * 2 + j).wait_recv()
+            for r in range(2):
+                rows = pl.ds(q * 8 * 2 + j * 8 + r * 4, 4)
+                s1[n, q * 4 + j * 2 + r] = wbuf[n, rows, c] + got_w[n, rows]
+
+        loop(2, tile)
+        ya_send(n, q).start()
+        yb_send(n, q).start()
 
     def pair_sum(n):
-        def tile(q):
-            pair_send(n, q).wait_recv()
-            for r in range(2):
-                rows = pl.ds(q * 8 + r * 4, 4)
-                pair = wbuf[n, rows, c].astype(F32) + got_w[n, rows].astype(F32)
-                s1[n, q * 2 + r] = pair.astype(BF)
-
-        loop(4, tile)
-        for q in (0, 1):
-            ya_send(n, q).start()
-        for q in (0, 1):
-            yb_send(n, q).start()
+        pair_half(n, 0)
+        pair_half(n, 1)
 
     def y_pass(n):
         for q in (0, 1):
             ya_send(n, q).wait_recv()
             rows, line = pl.ds(q * 4, 4), y_way(q)[0]
-            pair = s1[n, rows, line].astype(F32) + got_y[0, n, rows].astype(F32)
-            s1[n, rows, line] = pair.astype(BF)
+            s1[n, rows, line] = s1[n, rows, line] + got_y[0, n, rows]
             yc_send(n, q).start()
 
     def y_sum(n):
@@ -326,6 +333,13 @@
 
     def c_send(i):
         return remote(part.at[2, i], got_c.at[i], cs.at[i], cr.at[i], {"tp": toward(i)[0]})
+
+    def partial(i, block):
+        rows = pl.ds(pl.multiple_of(i * T, T), T)
+        span = pl.ds(pl.multiple_of(block * 512, 512), 512)
+        return rows_product(gb[rows, 0:256], wv[span, :]) + rows_product(
+            gb[rows, 256:512], wg[span, :]
+        )
 
     def back_tile(i):
         for h in range(2):
@@ -348,67 +362,62 @@
 
             loop(T // R, block)
 
-        rows = pl.ds(pl.multiple_of(i * T, T), T)
-
-        def partial(block):
-            span = pl.ds(pl.multiple_of(block * 512, 512), 512)
-            return rows_product(gb[rows, 0:256], wv[span, :]) + rows_product(
-                gb[rows, 256:512], wg[span, :]
-            )
-
-        near, back = toward(i)
-        part[0, i] = partial(far).astype(BF)
+        part[0, i] = partial(i, far).astype(BF)
         a_send(i).start()
-        part[1, i] = partial(back).astype(BF)
+        part[1, i] = partial(i, toward(i)[1]).astype(BF)
         b_send(i).start()
-        part[2, i] = partial(near).astype(BF)
-        own[i] = partial(t)
+
+    def near_tile(i):
+        part[2, i] = partial(i, toward(i)[0]).astype(BF)
+        own[i] = partial(i, t)
 
     def combine(i):
         a_send(i).wait_recv()
-        part[2, i] = (part[2, i].astype(F32) + got_a[i].astype(F32)).astype(BF)
+        part[2, i] = part[2, i] + got_a[i]
         c_send(i).start()
+
+    def gather(i):
+        b_send(i).wait_recv()
+        own[i] = own[i] + got_b[i].astype(F32)
 
     def pair(first, body):
         loop(2, lambda j: body(first + j))
 
     for copy in loads:
         copy.wait()
-    project(3)
+    loop(TILES, lambda j: project((j + 3) % 4))
+    filter_rows(1)
     pl.semaphore_wait(barrier, len(peers))
     halo_send.start()
-    loop(3, project)
+    filter_tell(1)
+    pair(2, filter_tile)
     for copy in late:
         copy.wait()
-    pair(0, mixed)
+    pair(1, mixed)
     halo_send.wait_recv()
     gi[:, 0:32, :] = jnp.where(s == 0, 0.0, gi_halo[...])
-    loop(TILES, filter_tile)
-    pair(2, mixed)
-    loop(TILES, activate)
+    filter_tile(0)
+    pair(1, activate)
+    loop(2, lambda j: mixed((j + 3) % 4))
+    loop(2, lambda j: activate((j + 3) % 4))
     proj_half(0)
-    filtered_grad(0)
-    grad_send.start()
+    pair(1, filtered_grad)
 
     def middle(j):
-        @pl.when(j < 3)
-        def _():
-            filtered_grad(j + 1)
-
         @pl.when(j == 1)
         def _():
             proj_half(2)
-
-        @pl.when(j == 2)
+            filtered_grad(3)
+            filtered_grad(0)
+            grad_send.start()
+
+        @pl.when(j == 3)
         def _():
             pair_sum(0)
-
-        @pl.when(j == 3)
-        def _():
             grad_send.wait_recv()
             gf[:, 1024:1056, :] = jnp.where(s == last_sp, 0.0, gf_halo[...])
 
-        back_tile(j)
+        back_tile(jnp.where(j == 3, 3, (j + 1) % 3))
 
     loop(TILES, middle)
 
@@ -420,15 +429,18 @@
     sm_pair = remote(smb.at[1 - c], sm_c, ms.at[0], mr.at[0], partner)
     sm_pair.start()
     y_pass(0)
-    gate_chunks()
+    gate_chunks(0, 3)
+    loop(2, lambda j: pair_half(j + 1, 0))
+    gate_chunks(3, 1)
+    loop(TILES, near_tile)
     sm_pair.wait_recv()
     smb[2] = smb[c] + sm_c[...]
     sm_ys = [remote(smb.at[2], sm_y.at[k - 1], ms.at[k], mr.at[k], at_y(k)) for k in (1, 2, 3)]
     for copy in sm_ys:
         copy.start()
-    loop(2, lambda j: pair_sum(j + 1))
+    loop(2, lambda j: pair_half(j + 1, 1))
     y_sum(0)
-    combine(0)
+    combine(1)
     for copy in sm_ys:
         copy.wait_recv()
     smb[3] = smb[2] + sm_y[0] + sm_y[1] + sm_y[2]
@@ -438,9 +450,9 @@
     for copy in sm_zs:
         copy.start()
     y_pass(1)
-    combine(1)
+    combine(2)
     y_pass(2)
-    combine(2)
+    combine(0)
     y_sum(1)
     y_sum(2)
     combine(3)
@@ -452,6 +464,7 @@
     smb[4] = total * scale
     sm_swap = remote(smb.at[4], smb.at[5], ms.at[11], mr.at[11], partner)
     sm_swap.start()
+    loop(TILES, gather)
     z_sum(0)
     sm_swap.wait_recv()
     sm_out[c] = smb[4]
@@ -459,12 +472,11 @@
     loop(2, lambda j: z_sum(j + 1))
 
     def finish(i):
-        b_send(i).wait_recv()
         c_send(i).wait_recv()
         rows = pl.ds(i * T, T)
-        ig_out[rows, :] = (own[i] + got_b[i].astype(F32) + got_c[i].astype(F32)).astype(BF)
-
-    for i in (0, 2, 1, 3):
+        ig_out[rows, :] = (own[i] + got_c[i].astype(F32)).astype(BF)
+
+    for i in (1, 2, 0, 3):
         finish(i)
 
     halo_send.wait_send()

time: 64.8 us -> 62.8 us (0.969)
  Pallas kernels: 64 us -> 62 us
    pallas_call x1, Pallas kernels: 61.9 us -> 59.8 us  [module(): pl.pallas_call(functools.partial(whole, scale), out_shape=(jax.ShapeDtype...]
where the time goes in v5:
time: 62.8 us; the launch traced here: 62.6 us
  Pallas kernels  62 us (99%)
  between operations  0.64 us (1%)
    pallas_call x1, Pallas kernels, module(): pl.pallas_call(functools.partial(whole, scale), out_shape=(jax.ShapeDtype...  59.8 us
    pallas_call x1, Pallas kernels, shards(): pl.pallas_call(placed, grid=(2,), in_specs=[pl.BlockSpec((512, 512), lamb...  2.13 us

profile of v5, /device:TPU:1, one launch (start us, length us, event | category | flops | bytes accessed | tf_op | source)
XLA Modules:
  0.0 62.6 jit_solution(17972729222885888414)
XLA Ops:
  0.6 59.8 %shard_map.135 = (bf16[1024,512]{1,0:T(8,128)(2,1)}, f32[3,32,256]{2,1,0:T(8,128)}, f32[2,40,128]{2,1,0:T(8,128)}) custom-call(bf16[1024,2048]{1,0:T(8,128)(2,1)} %x_h.1, bf16[1024,2048]{1,0:T(8,128)(2,1)} %g_h.1, bf16[2048,256]{1,0:T(8,128)(2,1)} %wv_h.1, bf16[2048,256]{1,0:T(8,128)(2,1)} %wg_h.1, f32[31,256]{1,0:T(8,128)} %taps.1, f32[1,256]{1,0:T(1,128)} %bitcast.6, ...), custom_call_target="tpu_custom_call" | custom-call | flops 10000000000 | bytes 14000000 | tf_op jit(solution)/shard_map/pallas_call | solution.py:516
  60.5 2.1 %shard_map.136 = (bf16[1024,512]{1,0:T(8,128)(2,1)}, f32[32,256]{1,0:T(8,128)}, f32[32,256]{1,0:T(8,128)}, f32[32,256]{1,0:T(8,128)}, f32[31,256]{1,0:T(8,128)}, /*index=5*/f32[1,256]{1,0:T(1,128)}, f32[1,256]{1,0:T(1,128)}) custom-call(bf16[1024,512]{1,0:T(8,128)(2,1)} %get-tuple-element.17.ig, f32[3,32,256]{2,1,0:T(8,128)} %get-tuple-element.18.w, ...), custom_call_target="tpu_custom_call" | custom-call | flops 1000000 | bytes 2000000 | tf_op jit(solution)/shard_map/pallas_call | solution.py:588

commit v6 on v5

--- a/solution.py
+++ b/solution.py
@@ -18,6 +18,7 @@
 T = 256
 TILES = 4
 R = 64
+FAR_FIRST = (4, 3, 5, 2, 6, 1, 7)
 
 
 def plain(left, right):
@@ -210,7 +211,7 @@
         loop(T // R, block)
         st2[i, 0:1] = token_sums(sum_a)
         st2[i, 1:2] = token_sums(sum_b)
-        for k in (1, 2, 3):
+        for k in (2, 1, 3):
             st2_send(i, k).start()
 
     def pair_send(n, q):
@@ -292,7 +293,7 @@
             yc_send(n, q).wait_recv()
         total = s1[n, :, y].astype(F32) + got_y[1, n].astype(F32) + got_y[2, n].astype(F32)
         s2[n] = total.astype(BF)
-        for k in range(1, 8):
+        for k in FAR_FIRST:
             z_send(n, k).start()
 
     def z_sum(n):
@@ -435,7 +436,7 @@
     loop(TILES, near_tile)
     sm_pair.wait_recv()
     smb[2] = smb[c] + sm_c[...]
-    sm_ys = [remote(smb.at[2], sm_y.at[k - 1], ms.at[k], mr.at[k], at_y(k)) for k in (1, 2, 3)]
+    sm_ys = [remote(smb.at[2], sm_y.at[k - 1], ms.at[k], mr.at[k], at_y(k)) for k in (2, 1, 3)]
     for copy in sm_ys:
         copy.start()
     loop(2, lambda j: pair_half(j + 1, 1))
@@ -445,7 +446,7 @@
         copy.wait_recv()
     smb[3] = smb[2] + sm_y[0] + sm_y[1] + sm_y[2]
     sm_zs = [
-        remote(smb.at[3], sm_z.at[k - 1], ms.at[3 + k], mr.at[3 + k], at_z(k)) for k in range(1, 8)
+        remote(smb.at[3], sm_z.at[k - 1], ms.at[3 + k], mr.at[3 + k], at_z(k)) for k in FAR_FIRST
     ]
     for copy in sm_zs:
         copy.start()

time: 62.8 us -> 62.8 us (level)
  no operation moved by 1% of the time
where the time goes in v6:
time: 62.8 us; the launch traced here: 62.6 us
  Pallas kernels  62 us (99%)
  between operations  0.64 us (1%)
    pallas_call x1, Pallas kernels, module(): pl.pallas_call(functools.partial(whole, scale), out_shape=(jax.ShapeDtype...  59.8 us
    pallas_call x1, Pallas kernels, shards(): pl.pallas_call(placed, grid=(2,), in_specs=[pl.BlockSpec((512, 512), lamb...  2.13 us

profile of v6, /device:TPU:1, one launch (start us, length us, event | category | flops | bytes accessed | tf_op | source)
XLA Modules:
  0.0 62.6 jit_solution(15031256315639446856)
XLA Ops:
  0.6 59.8 %shard_map.135 = (bf16[1024,512]{1,0:T(8,128)(2,1)}, f32[3,32,256]{2,1,0:T(8,128)}, f32[2,40,128]{2,1,0:T(8,128)}) custom-call(bf16[1024,2048]{1,0:T(8,128)(2,1)} %x_h.1, bf16[1024,2048]{1,0:T(8,128)(2,1)} %g_h.1, bf16[2048,256]{1,0:T(8,128)(2,1)} %wv_h.1, bf16[2048,256]{1,0:T(8,128)(2,1)} %wg_h.1, f32[31,256]{1,0:T(8,128)} %taps.1, f32[1,256]{1,0:T(1,128)} %bitcast.6, ...), custom_call_target="tpu_custom_call" | custom-call | flops 10000000000 | bytes 14000000 | tf_op jit(solution)/shard_map/pallas_call | solution.py:517
  60.5 2.1 %shard_map.136 = (bf16[1024,512]{1,0:T(8,128)(2,1)}, f32[32,256]{1,0:T(8,128)}, f32[32,256]{1,0:T(8,128)}, f32[32,256]{1,0:T(8,128)}, f32[31,256]{1,0:T(8,128)}, /*index=5*/f32[1,256]{1,0:T(1,128)}, f32[1,256]{1,0:T(1,128)}) custom-call(bf16[1024,512]{1,0:T(8,128)(2,1)} %get-tuple-element.17.ig, f32[3,32,256]{2,1,0:T(8,128)} %get-tuple-element.18.w, ...), custom_call_target="tpu_custom_call" | custom-call | flops 1000000 | bytes 2000000 | tf_op jit(solution)/shard_map/pallas_call | solution.py:589
